TPU v7x, 32 devices: a whole 2x2x4 slice. The times are simulated.
32 devices in a mesh: ep: 8 (over z, x), tp: 4 (over y, core).
Axes of the slice: x: 2, y: 2, z: 4, core: 2. Of those that a mesh axis runs over, the one named last changes fastest.
Arguments:
- queries: bfloat16 [3072, 2048], P('ep', 'tp'), may hold values from -8 to 8
- keys: bfloat16 [3072, 2048], P('ep', 'tp'), may hold values from -8 to 8
- values: bfloat16 [3072, 2048], P('ep', 'tp'), may hold values from -6 to 6
- key_offset: bfloat16 [3072, 16], P('ep', 'tp'), may hold values from -15.25 to -0.4
- rows: bfloat16 [1024, 2048], P('ep'), may hold values from -6 to 6
- gain: float32 [2048], replicated, may hold values from 0.1 to 1.9
- gate_w: bfloat16 [8, 2048, 3584], P('ep', None, 'tp'), may hold values from -0.125 to 0.125
- up_w: bfloat16 [8, 2048, 3584], P('ep', None, 'tp'), may hold values from -0.125 to 0.125
- down_w: bfloat16 [8, 3584, 2048], P('ep', 'tp'), may hold values from -0.09375 to 0.09375
- expert_ids: int32 [1024, 2], P('ep'), may hold values from 0 to 7, all different within a row; in each aligned block of 128 rows (0 to 127, 128 to 255, ...) at most 64 rows name the same one
- route_weights: float32 [1024, 2], P('ep'), may hold values from 0.2 to 1
Outputs:
- attended: bfloat16 [3072, 2048], P('ep', 'tp')
- mixed: bfloat16 [1024, 2048], P('ep')
Inputs may be any that keep to these rules, and one draw needn't show every extreme that they name: `expert_ids`: each token names 2 different experts; among the 128 tokens of one ep index no expert is chosen more than 64 times, and in some such block an expert is chosen exactly 64 times.
All inputs are finite; a program needn't handle non-finite values.
Results may differ from a plain program's by a relative error of at most 0.019.
Values may be sent and summed in bfloat16 or wider, within the bound.
A program may use at most 128 MiB of HBM per device.

v0:
```python
import jax
import jax.numpy as jnp
from jax import lax
from jax.sharding import PartitionSpec as P

EPSILON = 1e-06


def stick_mixer(queries, keys, values, key_offset):
    position = lax.axis_index("ep")
    query_len = queries.shape[0]
    heads = key_offset.shape[1]
    head_dim = queries.shape[1] // heads
    scale = head_dim ** (-0.5)
    query_heads = queries.reshape(query_len, heads, head_dim)
    query_pos = position * query_len + jnp.arange(query_len, dtype=jnp.int32)
    last_row = (position + 1) * query_len
    key_piece = lax.all_gather(keys, "ep", axis=0, tiled=True)
    value_piece = lax.all_gather(values, "ep", axis=0, tiled=True)
    offset_piece = lax.all_gather(key_offset, "ep", axis=0, tiled=True)
    block_count = key_piece.shape[0] // query_len
    key_split = key_piece.reshape(block_count, query_len, heads, head_dim)
    value_split = value_piece.reshape(block_count, query_len, heads, head_dim)
    offset_split = offset_piece.reshape(block_count, query_len, heads)

    def compute_block(key_here, value_here, offset_here, key_start):
        key_pos = key_start + jnp.arange(query_len, dtype=jnp.int32)
        logits = (
            jnp.einsum("qhd,khd->hqk", query_heads, key_here, preferred_element_type=jnp.float32)
            * scale
        )
        logits = logits + offset_here.astype(jnp.float32).T[:, None, :]
        strict = key_pos[None, None, :] < query_pos[None, :, None]
        breaks = jnp.where(strict, jax.nn.log_sigmoid(-logits), 0.0)
        within = lax.cumsum(breaks, axis=2, reverse=True) - breaks
        local = jnp.where(strict, jnp.exp(jax.nn.log_sigmoid(logits) + within), 0.0).astype(
            jnp.bfloat16
        )
        summed = jnp.einsum("hqk,khd->hqd", local, value_here, preferred_element_type=jnp.float32)
        return (summed, jnp.sum(breaks, axis=2))

    def skip_block(key_here, value_here, offset_here, key_start):
        return (
            jnp.zeros((heads, query_len, head_dim), jnp.float32),
            jnp.zeros((heads, query_len), jnp.float32),
        )

    def one_block(args):
        key_here, value_here, offset_here, block_index = args
        key_start = block_index * query_len
        return lax.cond(
            key_start < last_row,
            compute_block,
            skip_block,
            key_here,
            value_here,
            offset_here,
            key_start,
        )

    sums, totals = lax.map(
        one_block, (key_split, value_split, offset_split, jnp.arange(block_count, dtype=jnp.int32))
    )
    sums, totals = (sums, totals)
    later = lax.cumsum(totals, axis=0, reverse=True) - totals
    combined = jnp.einsum("bhq,bhqd->qhd", jnp.exp(later), sums, precision=lax.Precision.HIGHEST)
    return combined.reshape(query_len, heads * head_dim).astype(jnp.bfloat16)


def routed_experts(rows, gain, gate_w, up_w, down_w, expert_ids, route_weights):
    ep_count = lax.axis_size("ep")
    local_experts = gate_w.shape[0]
    experts_all = ep_count * local_experts
    token_count = rows.shape[0]
    choose_count = expert_ids.shape[1]
    width = rows.shape[1]
    capacity = 2 * choose_count * token_count // experts_all
    rows_float = rows.astype(jnp.float32)
    normed = rows_float * lax.rsqrt(
        jnp.mean(rows_float * rows_float, axis=1, keepdims=True) + EPSILON
    )
    normed = (normed * gain[None, :]).astype(jnp.bfloat16)
    flat_ids = expert_ids.reshape(-1)
    onehot = (flat_ids[:, None] == jnp.arange(experts_all, dtype=jnp.int32)[None, :]).astype(
        jnp.int32
    )
    ranked = jnp.sum((jnp.cumsum(onehot, axis=0) - onehot) * onehot, axis=1)
    token_of = jnp.arange(token_count * choose_count, dtype=jnp.int32) // choose_count
    source_rows = (
        jnp.zeros((experts_all * capacity,), jnp.int32)
        .at[flat_ids * capacity + ranked]
        .set(token_of)
    )
    outgoing = normed[source_rows].reshape(ep_count, local_experts, capacity, width)
    arrived = lax.all_to_all(outgoing, "ep", split_axis=0, concat_axis=0, tiled=True)
    gate_val = jnp.einsum("sxcd,xdf->csxf", arrived, gate_w, preferred_element_type=jnp.float32)
    up_val = jnp.einsum("sxcd,xdf->csxf", arrived, up_w, preferred_element_type=jnp.float32)
    hidden = (jax.nn.silu(gate_val) * up_val).astype(jnp.bfloat16)
    share = lax.psum_scatter(
        jnp.einsum("csxf,xfd->csxd", hidden, down_w, preferred_element_type=jnp.float32).astype(
            jnp.bfloat16
        ),
        "tp",
        scatter_dimension=0,
        tiled=True,
    )
    returned = lax.all_to_all(share, "ep", split_axis=1, concat_axis=1, tiled=True)
    whole_slots = lax.all_gather(returned, "tp", axis=0, tiled=True)
    flat_out = whole_slots.reshape(capacity * experts_all, width)
    slot_index = ranked * experts_all + flat_ids
    picked = flat_out[slot_index].astype(jnp.float32).reshape(token_count, choose_count, width)
    return jnp.sum(picked * route_weights[:, :, None], axis=1).astype(jnp.bfloat16)


def body(
    queries, keys, values, key_offset, rows, gain, gate_w, up_w, down_w, expert_ids, route_weights
):
    attended = stick_mixer(queries, keys, values, key_offset)
    mixed = routed_experts(rows, gain, gate_w, up_w, down_w, expert_ids, route_weights)
    return (attended, mixed)


def solution(mesh):
    in_specs = (
        P("ep", "tp"),
        P("ep", "tp"),
        P("ep", "tp"),
        P("ep", "tp"),
        P("ep", None),
        P(),
        P("ep", None, "tp"),
        P("ep", None, "tp"),
        P("ep", "tp", None),
        P("ep", None),
        P("ep", None),
    )
    out_specs = (P("ep", "tp"), P("ep", None))
    return jax.shard_map(body, mesh=mesh, in_specs=in_specs, out_specs=out_specs, check_vma=False)
```

profile of v0, /device:TPU:27, one launch (start us, length us, event | category | flops | bytes accessed | tf_op | source)
XLA Modules:
  0.0 671.1 jit_solution(18200842796878215469)
XLA Ops:
  16.6 51.5 %all_to_all.10 = bf16[8,1,64,2048]{3,2,1,0:T(8,128)(2,1)S(1)} all-to-all(bf16[8,1,64,2048]{3,2,1,0:T(8,128)(2,1)S(1)} %bitcast.147), channel_id=1, replica_groups=mesh['ep'=8,'tp'=4] {'ep'}, dimensions={0} | all-to-all | bytes 4194304 | tf_op jit(solution)/shard_map/all_to_all | solution.py:95
  72.9 3.8 fusion.32
  78.0 31.2 %reduce-scatter.2.cloned.1.call-done = bf16[16,8,1,2048]{3,1,0,2:T(8,128)(2,1)} async-done(((bf16[64,8,1,2048]{3,1,0,2:T(8,128)(2,1)}), bf16[16,8,1,2048]{3,1,0,2:T(8,128)(2,1)}) %reduce-scatter.2.cloned.1.call-update) | async-done | bytes 524304 | tf_op jit(solution)/shard_map/reduce_scatter | solution.py:99
  110.6 32.5 %all_to_all.11 = bf16[16,8,1,2048]{3,0,2,1:T(8,128)(2,1)S(1)} all-to-all(bf16[16,8,1,2048]{3,0,2,1:T(8,128)(2,1)S(1)} %copy.46), channel_id=1, replica_groups=mesh['ep'=8,'tp'=4] {'ep'}, dimensions={1} | all-to-all | bytes 1048576 | tf_op jit(solution)/shard_map/all_to_all | solution.py:107
  145.5 24.5 %all_gather.13 = bf16[3072,4]{0,1:T(4,128)(2,1)S(1)} all-gather(bf16[384,4]{0,1:T(4,128)(2,1)S(1)} %copy-done.2), channel_id=1, replica_groups=mesh['ep'=8,'tp'=4] {'ep'}, dimensions={0}, use_global_device_ids=true | all-gather | bytes 27648 | tf_op jit(solution)/shard_map/all_gather | solution.py:20
  170.0 3.8 reshape.234
  176.3 32.6 %all-gather.6.cloned.1.call-done = bf16[3072,512]{1,0:T(8,128)(2,1)} async-done(((bf16[384,512]{1,0:T(8,128)(2,1)}), bf16[3072,512]{1,0:T(8,128)(2,1)}) %all-gather.6.cloned.1.call-update) | async-done | bytes 3145744 | tf_op jit(solution)/shard_map/all_gather | solution.py:19
  208.9 3.8 reshape.235
  215.0 425.2 %while.13 = (s32[]{:T(128)}, f32[8,4,384,128]{3,0,1,2:T(8,128)}, f32[8,4,384]{2,1,0:T(4,128)S(1)}, s32[8]{0:T(128)S(1)}, s32[]{:T(128)}, /*index=5*/bf16[8,384,4...) while((s32[]{:T(128)}, f32[8,4,384,128]{3,0,1,2:T(8,128)}, ...), condition=%wide.region_6.7_spmd.clone, body=%wide.region_0.6_spmd.clone.sunk | while | flops 397112064 | bytes 41129264 | solution.py:61
  230.9 27.0 %conditional.3 = (f32[1,4,384,128]{3,2,1,0:T(8,128)}, f32[1,4,384]{2,1,0:T(4,128)S(1)}) conditional(s32[]{:T(128)} %convert_element_type.93, () %tuple.51, (s32[]{:T(128)}, s32[]{:T(128)}, bf16[8,384,4,128]{3,1,2,0:T(8,128)(2,1)}, s32[]{:T(128)}, bf16[384,4,128]{2,0,1:T(8,128)(2,1)}, /*index=5*/bf16[8,384,4]{1,2,0:T(4,128)(2,1)S(1)}, ...), branch_computations={%region_1.1_spmd, %region_2.5_spmd} | conditional | flops 397112064 | bytes 37969468 | solution.py:51
  231.1 4.4 fusion.22
  235.5 14.0 %fusion.2 = f32[4,384,3,128]{1,2,3,0:T(4,128)S(1)} fusion(f32[4,384,3,128]{1,3,2,0:T(8,128)S(1)} %bitcast.145), kind=kOutput, calls=%fused_computation.6 | output fusion | flops 74907648 | bytes 4718592 | tf_op jit(solution)/shard_map/reduce-window.6
  251.8 3.6 fusion.8
  259.9 21.0 %dynamic_update_slice.14 = f32[8,4,384,128]{3,0,1,2:T(8,128)} dynamic-update-slice(f32[8,4,384,128]{3,0,1,2:T(8,128)} %get-tuple-element.285, f32[1,4,384,128]{3,0,1,2:T(1,128)S(1)} %copy.70, s32[]{:T(128)} %copy.80, s32[]{:T(128)} %constant.84.clone.1..sunk, s32[]{:T(128)} %constant.84.clone.1..sunk, s32[]{:T(128)} %constant.84.clone.1..sunk) | dynamic-update-slice | bytes 1572868 | tf_op jit(solution)/shard_map/while/body/jit(dynamic_update_index_in_dim)/dynamic_update_slice | solution.py:61
  282.2 27.0 %conditional.3 = (f32[1,4,384,128]{3,2,1,0:T(8,128)}, f32[1,4,384]{2,1,0:T(4,128)S(1)}) conditional(s32[]{:T(128)} %convert_element_type.93, () %tuple.51, (s32[]{:T(128)}, s32[]{:T(128)}, bf16[8,384,4,128]{3,1,2,0:T(8,128)(2,1)}, s32[]{:T(128)}, bf16[384,4,128]{2,0,1:T(8,128)(2,1)}, /*index=5*/bf16[8,384,4]{1,2,0:T(4,128)(2,1)S(1)}, ...), branch_computations={%region_1.1_spmd, %region_2.5_spmd} | conditional | flops 397112064 | bytes 37969468 | solution.py:51
  282.4 4.4 fusion.22
  286.8 14.0 %fusion.2 = f32[4,384,3,128]{1,2,3,0:T(4,128)S(1)} fusion(f32[4,384,3,128]{1,3,2,0:T(8,128)S(1)} %bitcast.145), kind=kOutput, calls=%fused_computation.6 | output fusion | flops 74907648 | bytes 4718592 | tf_op jit(solution)/shard_map/reduce-window.6
  303.1 3.6 fusion.8
  311.2 21.0 %dynamic_update_slice.14 = f32[8,4,384,128]{3,0,1,2:T(8,128)} dynamic-update-slice(f32[8,4,384,128]{3,0,1,2:T(8,128)} %get-tuple-element.285, f32[1,4,384,128]{3,0,1,2:T(1,128)S(1)} %copy.70, s32[]{:T(128)} %copy.80, s32[]{:T(128)} %constant.84.clone.1..sunk, s32[]{:T(128)} %constant.84.clone.1..sunk, s32[]{:T(128)} %constant.84.clone.1..sunk) | dynamic-update-slice | bytes 1572868 | tf_op jit(solution)/shard_map/while/body/jit(dynamic_update_index_in_dim)/dynamic_update_slice | solution.py:61
  333.6 27.0 %conditional.3 = (f32[1,4,384,128]{3,2,1,0:T(8,128)}, f32[1,4,384]{2,1,0:T(4,128)S(1)}) conditional(s32[]{:T(128)} %convert_element_type.93, () %tuple.51, (s32[]{:T(128)}, s32[]{:T(128)}, bf16[8,384,4,128]{3,1,2,0:T(8,128)(2,1)}, s32[]{:T(128)}, bf16[384,4,128]{2,0,1:T(8,128)(2,1)}, /*index=5*/bf16[8,384,4]{1,2,0:T(4,128)(2,1)S(1)}, ...), branch_computations={%region_1.1_spmd, %region_2.5_spmd} | conditional | flops 397112064 | bytes 37969468 | solution.py:51
  333.8 4.4 fusion.22
  338.2 14.0 %fusion.2 = f32[4,384,3,128]{1,2,3,0:T(4,128)S(1)} fusion(f32[4,384,3,128]{1,3,2,0:T(8,128)S(1)} %bitcast.145), kind=kOutput, calls=%fused_computation.6 | output fusion | flops 74907648 | bytes 4718592 | tf_op jit(solution)/shard_map/reduce-window.6
  354.5 3.6 fusion.8
  362.6 21.0 %dynamic_update_slice.14 = f32[8,4,384,128]{3,0,1,2:T(8,128)} dynamic-update-slice(f32[8,4,384,128]{3,0,1,2:T(8,128)} %get-tuple-element.285, f32[1,4,384,128]{3,0,1,2:T(1,128)S(1)} %copy.70, s32[]{:T(128)} %copy.80, s32[]{:T(128)} %constant.84.clone.1..sunk, s32[]{:T(128)} %constant.84.clone.1..sunk, s32[]{:T(128)} %constant.84.clone.1..sunk) | dynamic-update-slice | bytes 1572868 | tf_op jit(solution)/shard_map/while/body/jit(dynamic_update_index_in_dim)/dynamic_update_slice | solution.py:61
  384.9 27.0 %conditional.3 = (f32[1,4,384,128]{3,2,1,0:T(8,128)}, f32[1,4,384]{2,1,0:T(4,128)S(1)}) conditional(s32[]{:T(128)} %convert_element_type.93, () %tuple.51, (s32[]{:T(128)}, s32[]{:T(128)}, bf16[8,384,4,128]{3,1,2,0:T(8,128)(2,1)}, s32[]{:T(128)}, bf16[384,4,128]{2,0,1:T(8,128)(2,1)}, /*index=5*/bf16[8,384,4]{1,2,0:T(4,128)(2,1)S(1)}, ...), branch_computations={%region_1.1_spmd, %region_2.5_spmd} | conditional | flops 397112064 | bytes 37969468 | solution.py:51
  385.1 4.4 fusion.22
  389.5 14.0 %fusion.2 = f32[4,384,3,128]{1,2,3,0:T(4,128)S(1)} fusion(f32[4,384,3,128]{1,3,2,0:T(8,128)S(1)} %bitcast.145), kind=kOutput, calls=%fused_computation.6 | output fusion | flops 74907648 | bytes 4718592 | tf_op jit(solution)/shard_map/reduce-window.6
  405.8 3.6 fusion.8
  413.9 21.0 %dynamic_update_slice.14 = f32[8,4,384,128]{3,0,1,2:T(8,128)} dynamic-update-slice(f32[8,4,384,128]{3,0,1,2:T(8,128)} %get-tuple-element.285, f32[1,4,384,128]{3,0,1,2:T(1,128)S(1)} %copy.70, s32[]{:T(128)} %copy.80, s32[]{:T(128)} %constant.84.clone.1..sunk, s32[]{:T(128)} %constant.84.clone.1..sunk, s32[]{:T(128)} %constant.84.clone.1..sunk) | dynamic-update-slice | bytes 1572868 | tf_op jit(solution)/shard_map/while/body/jit(dynamic_update_index_in_dim)/dynamic_update_slice | solution.py:61
  436.2 27.0 %conditional.3 = (f32[1,4,384,128]{3,2,1,0:T(8,128)}, f32[1,4,384]{2,1,0:T(4,128)S(1)}) conditional(s32[]{:T(128)} %convert_element_type.93, () %tuple.51, (s32[]{:T(128)}, s32[]{:T(128)}, bf16[8,384,4,128]{3,1,2,0:T(8,128)(2,1)}, s32[]{:T(128)}, bf16[384,4,128]{2,0,1:T(8,128)(2,1)}, /*index=5*/bf16[8,384,4]{1,2,0:T(4,128)(2,1)S(1)}, ...), branch_computations={%region_1.1_spmd, %region_2.5_spmd} | conditional | flops 397112064 | bytes 37969468 | solution.py:51
  436.4 4.4 fusion.22
  440.8 14.0 %fusion.2 = f32[4,384,3,128]{1,2,3,0:T(4,128)S(1)} fusion(f32[4,384,3,128]{1,3,2,0:T(8,128)S(1)} %bitcast.145), kind=kOutput, calls=%fused_computation.6 | output fusion | flops 74907648 | bytes 4718592 | tf_op jit(solution)/shard_map/reduce-window.6
  465.2 21.0 %dynamic_update_slice.14 = f32[8,4,384,128]{3,0,1,2:T(8,128)} dynamic-update-slice(f32[8,4,384,128]{3,0,1,2:T(8,128)} %get-tuple-element.285, f32[1,4,384,128]{3,0,1,2:T(1,128)S(1)} %copy.70, s32[]{:T(128)} %copy.80, s32[]{:T(128)} %constant.84.clone.1..sunk, s32[]{:T(128)} %constant.84.clone.1..sunk, s32[]{:T(128)} %constant.84.clone.1..sunk) | dynamic-update-slice | bytes 1572868 | tf_op jit(solution)/shard_map/while/body/jit(dynamic_update_index_in_dim)/dynamic_update_slice | solution.py:61
  487.6 27.0 %conditional.3 = (f32[1,4,384,128]{3,2,1,0:T(8,128)}, f32[1,4,384]{2,1,0:T(4,128)S(1)}) conditional(s32[]{:T(128)} %convert_element_type.93, () %tuple.51, (s32[]{:T(128)}, s32[]{:T(128)}, bf16[8,384,4,128]{3,1,2,0:T(8,128)(2,1)}, s32[]{:T(128)}, bf16[384,4,128]{2,0,1:T(8,128)(2,1)}, /*index=5*/bf16[8,384,4]{1,2,0:T(4,128)(2,1)S(1)}, ...), branch_computations={%region_1.1_spmd, %region_2.5_spmd} | conditional | flops 397112064 | bytes 37969468 | solution.py:51
  487.8 4.4 fusion.22
  492.2 14.0 %fusion.2 = f32[4,384,3,128]{1,2,3,0:T(4,128)S(1)} fusion(f32[4,384,3,128]{1,3,2,0:T(8,128)S(1)} %bitcast.145), kind=kOutput, calls=%fused_computation.6 | output fusion | flops 74907648 | bytes 4718592 | tf_op jit(solution)/shard_map/reduce-window.6
  516.6 21.0 %dynamic_update_slice.14 = f32[8,4,384,128]{3,0,1,2:T(8,128)} dynamic-update-slice(f32[8,4,384,128]{3,0,1,2:T(8,128)} %get-tuple-element.285, f32[1,4,384,128]{3,0,1,2:T(1,128)S(1)} %copy.70, s32[]{:T(128)} %copy.80, s32[]{:T(128)} %constant.84.clone.1..sunk, s32[]{:T(128)} %constant.84.clone.1..sunk, s32[]{:T(128)} %constant.84.clone.1..sunk) | dynamic-update-slice | bytes 1572868 | tf_op jit(solution)/shard_map/while/body/jit(dynamic_update_index_in_dim)/dynamic_update_slice | solution.py:61
  538.9 27.0 %conditional.3 = (f32[1,4,384,128]{3,2,1,0:T(8,128)}, f32[1,4,384]{2,1,0:T(4,128)S(1)}) conditional(s32[]{:T(128)} %convert_element_type.93, () %tuple.51, (s32[]{:T(128)}, s32[]{:T(128)}, bf16[8,384,4,128]{3,1,2,0:T(8,128)(2,1)}, s32[]{:T(128)}, bf16[384,4,128]{2,0,1:T(8,128)(2,1)}, /*index=5*/bf16[8,384,4]{1,2,0:T(4,128)(2,1)S(1)}, ...), branch_computations={%region_1.1_spmd, %region_2.5_spmd} | conditional | flops 397112064 | bytes 37969468 | solution.py:51
  539.1 4.4 fusion.22
  543.5 14.0 %fusion.2 = f32[4,384,3,128]{1,2,3,0:T(4,128)S(1)} fusion(f32[4,384,3,128]{1,3,2,0:T(8,128)S(1)} %bitcast.145), kind=kOutput, calls=%fused_computation.6 | output fusion | flops 74907648 | bytes 4718592 | tf_op jit(solution)/shard_map/reduce-window.6
  567.9 21.0 %dynamic_update_slice.14 = f32[8,4,384,128]{3,0,1,2:T(8,128)} dynamic-update-slice(f32[8,4,384,128]{3,0,1,2:T(8,128)} %get-tuple-element.285, f32[1,4,384,128]{3,0,1,2:T(1,128)S(1)} %copy.70, s32[]{:T(128)} %copy.80, s32[]{:T(128)} %constant.84.clone.1..sunk, s32[]{:T(128)} %constant.84.clone.1..sunk, s32[]{:T(128)} %constant.84.clone.1..sunk) | dynamic-update-slice | bytes 1572868 | tf_op jit(solution)/shard_map/while/body/jit(dynamic_update_index_in_dim)/dynamic_update_slice | solution.py:61
  590.2 27.0 %conditional.3 = (f32[1,4,384,128]{3,2,1,0:T(8,128)}, f32[1,4,384]{2,1,0:T(4,128)S(1)}) conditional(s32[]{:T(128)} %convert_element_type.93, () %tuple.51, (s32[]{:T(128)}, s32[]{:T(128)}, bf16[8,384,4,128]{3,1,2,0:T(8,128)(2,1)}, s32[]{:T(128)}, bf16[384,4,128]{2,0,1:T(8,128)(2,1)}, /*index=5*/bf16[8,384,4]{1,2,0:T(4,128)(2,1)S(1)}, ...), branch_computations={%region_1.1_spmd, %region_2.5_spmd} | conditional | flops 397112064 | bytes 37969468 | solution.py:51
  590.5 4.4 fusion.22
  594.8 14.0 %fusion.2 = f32[4,384,3,128]{1,2,3,0:T(4,128)S(1)} fusion(f32[4,384,3,128]{1,3,2,0:T(8,128)S(1)} %bitcast.145), kind=kOutput, calls=%fused_computation.6 | output fusion | flops 74907648 | bytes 4718592 | tf_op jit(solution)/shard_map/reduce-window.6
  619.2 21.0 %dynamic_update_slice.14 = f32[8,4,384,128]{3,0,1,2:T(8,128)} dynamic-update-slice(f32[8,4,384,128]{3,0,1,2:T(8,128)} %get-tuple-element.285, f32[1,4,384,128]{3,0,1,2:T(1,128)S(1)} %copy.70, s32[]{:T(128)} %copy.80, s32[]{:T(128)} %constant.84.clone.1..sunk, s32[]{:T(128)} %constant.84.clone.1..sunk, s32[]{:T(128)} %constant.84.clone.1..sunk) | dynamic-update-slice | bytes 1572868 | tf_op jit(solution)/shard_map/while/body/jit(dynamic_update_index_in_dim)/dynamic_update_slice | solution.py:61
  640.8 11.9 %fusion.61 = f32[384,4,1,128]{3,2,1,0:T(1,128)S(1)} fusion(f32[8,4,384,1]{0,3,1,2:T(1,128)S(1)} %copy.50, f32[8,4,384,128]{3,0,1,2:T(8,128)} %get-tuple-element.126), kind=kOutput, calls=%fused_computation.88 | convolution fusion | flops 18874368 | bytes 7127040 | tf_op jit(solution)/shard_map/bhq,bhqd->qhd/dot_general | solution.py:66
  653.6 4.2 gather_fusion.1
  659.2 3.9 multiply_reduce_fusion
  (183 shorter events, 100.7 us)
Async XLA Ops:
  8.0 101.2 %reduce-scatter.2.cloned.1.call-start = ((), (), s32[]{:S(2)}) async-start(), calls=%async_computation.5 | async-start | bytes 2621440 | tf_op jit(solution)/shard_map/reduce_scatter | solution.py:99
  16.6 51.6 %copy-start.4 = (bf16[1,2048,896]{2,1,0:T(8,128)(2,1)S(1)}, bf16[1,2048,896]{2,1,0:T(8,128)(2,1)}, u32[]{:S(2)}) copy-start(bf16[1,2048,896]{2,1,0:T(8,128)(2,1)} %param.21) | copy-start | bytes 11010052
  68.2 2.3 copy-start.5
  70.5 2.4 copy-start.6
  76.8 67.5 %copy-start.1 = (bf16[384,512]{1,0:T(8,128)(2,1)S(1)}, bf16[384,512]{1,0:T(8,128)(2,1)}, u32[]{:S(2)}) copy-start(bf16[384,512]{1,0:T(8,128)(2,1)} %param.15) | copy-start | bytes 1179652
  76.8 93.2 %all-gather.4.cloned.1.call-start = ((), (), s32[]{:S(2)}) async-start(), calls=%async_computation.3 | async-start | bytes 3538944 | tf_op jit(solution)/shard_map/all_gather | solution.py:18
  77.4 131.5 %all-gather.6.cloned.1.call-start = ((), (), s32[]{:S(2)}) async-start(), calls=%async_computation.4 | async-start | bytes 3538944 | tf_op jit(solution)/shard_map/all_gather | solution.py:19
  78.0 575.7 %all-gather.8.cloned.1.call-start = ((), (), s32[]{:S(2)}) async-start(), calls=%async_computation.6 | async-start | bytes 2621440 | tf_op jit(solution)/shard_map/all_gather | solution.py:108
  110.6 34.8 %copy-start.3 = (f32[128,2]{0,1:T(2,128)S(1)}, f32[128,2]{0,1:T(2,128)}, u32[]{:S(2)}) copy-start(f32[128,2]{0,1:T(2,128)} %param.25) | copy-start | bytes 3076
  110.6 34.9 %copy-start.2 = (bf16[384,4]{0,1:T(4,128)(2,1)S(1)}, bf16[384,4]{0,1:T(4,128)(2,1)}, u32[]{:S(2)}) copy-start(bf16[384,4]{0,1:T(4,128)(2,1)} %param.18) | copy-start | bytes 9220
  250.1 1.7 copy-start
  301.5 1.7 copy-start
  352.8 1.7 copy-start
  404.1 1.7 copy-start
  455.5 1.7 copy-start
  506.8 1.7 copy-start
  558.1 1.7 copy-start
  609.5 1.7 copy-start
Sparse Core Ops, SparseCore 0:
  76.9 32.2 reduce-scatter.1
Sparse Core Ops, SparseCore 1:
  79.5 68.8 all-gather.3
  150.4 58.4 all-gather.5
  210.9 23.9 all-gather.7
where the time goes:
time: 678 us; the launch traced here: 671 us
  local copies, waits for them, and re-layouts  230 us (34%)
  other arithmetic  155 us (23%)
  blocking collectives  109 us (16%)
  matrix products  75.4 us (11%)
  waiting for transfers between devices  64.9 us (10%)
  loops' own time  20.9 us (3%)
  between operations  16.3 us (2%)
    dynamic_update_slice x24, local copies, waits for them, and re-layouts, stick_mixer(): lax.map(one_block, (key_split, value_split, offset_split, jnp.arange(bloc...  183 us
    another operation x18, other arithmetic  113 us
    all_to_all x1, blocking collectives, routed_experts(): lax.all_to_all(outgoing, 'ep', split_axis=0, concat_axis=0, tiled=True)  51.5 us
    dot_general x8, matrix products, compute_block(): jnp.einsum('qhd,khd->hqk', query_heads, key_here, preferred_element_type=...  35 us
    all_gather x1, waiting for transfers between devices, stick_mixer(): value_piece = lax.all_gather(values, 'ep', axis=0, tiled=True)  32.6 us
    all_to_all x1, blocking collectives, routed_experts(): lax.all_to_all(share, 'ep', split_axis=1, concat_axis=1, tiled=True)  32.5 us
    reduce_scatter x1, waiting for transfers between devices, routed_experts(): lax.psum_scatter(jnp.einsum('csxf,xfd->csxd', hidden, down_w, preferred_e...  31.2 us
    convert_element_type x8, other arithmetic, compute_block(): jnp.where(strict, jnp.exp(jax.nn.log_sigmoid(logits) + within), 0.0)  29.1 us
  transfers between devices with their start and end apart: 4, of which 2 were waited for; matrix products, arithmetic and copies ran while one was open for 63% of the time, Pallas kernels for 0%

commit v1 on v0

v1 whole, which is shorter than its diff:
```python
import jax
import jax.numpy as jnp
from jax import lax
from jax.experimental import pallas as pl
from jax.experimental.pallas import tpu as pltpu
from jax.sharding import PartitionSpec as P

EPSILON = 1e-06


def stick_kernel(place_ref, q_ref, k_ref, v_ref, offset_ref, out_ref):
    rows, head_dim = q_ref.shape
    scale = head_dim ** (-0.5)
    place = place_ref[0]
    across = lax.broadcasted_iota(jnp.int32, (rows, rows), 0)
    along = lax.broadcasted_iota(jnp.int32, (rows, rows), 1)
    strict = along < across
    after = jnp.where(strict, 1.0, 0.0).astype(jnp.bfloat16)
    query = q_ref[...]

    def one_block(block, masked):
        here = pl.ds(pl.multiple_of(block * rows, rows), rows)
        logits = lax.dot_general(
            query, k_ref[here, :], (((1,), (1,)), ((), ())), preferred_element_type=jnp.float32
        )
        logits = logits * scale + offset_ref[0, pl.ds(block, 1), :]
        breaks = -(jnp.maximum(logits, 0.0) + jnp.log(1.0 + jnp.exp(-jnp.abs(logits))))
        chosen = logits + breaks
        if masked:
            breaks = jnp.where(strict, breaks, 0.0)
        within = jnp.dot(breaks.astype(jnp.bfloat16), after, preferred_element_type=jnp.float32)
        local = jnp.exp(chosen + within)
        if masked:
            local = jnp.where(strict, local, 0.0)
        summed = jnp.dot(
            local.astype(jnp.bfloat16), v_ref[here, :], preferred_element_type=jnp.float32
        )
        return summed, jnp.sum(breaks, axis=1, keepdims=True)

    def step(index, carry):
        total, later = carry
        summed, block_total = one_block(place - 1 - index, False)
        return total + jnp.exp(later) * summed, later + block_total

    total, _ = lax.fori_loop(0, place, step, one_block(place, True))
    out_ref[...] = total.astype(out_ref.dtype)


def stick_mixer(queries, keys, values, key_offset):
    query_len, width = queries.shape
    heads = key_offset.shape[1]
    head_dim = width // heads
    key_all = lax.all_gather(keys, "ep", axis=0, tiled=True)
    value_all = lax.all_gather(values, "ep", axis=0, tiled=True)
    offset_all = lax.all_gather(key_offset.T, "ep", axis=0)
    offset_all = jnp.swapaxes(offset_all, 0, 1).astype(jnp.float32)
    blocks = offset_all.shape[1]
    length = blocks * query_len
    place = lax.axis_index("ep").astype(jnp.int32).reshape(1)
    pairs = heads * blocks * query_len * query_len
    return pl.pallas_call(
        stick_kernel,
        grid=(heads,),
        in_specs=[
            pl.BlockSpec(memory_space=pltpu.SMEM),
            pl.BlockSpec((query_len, head_dim), lambda h: (0, h)),
            pl.BlockSpec((length, head_dim), lambda h: (0, h)),
            pl.BlockSpec((length, head_dim), lambda h: (0, h)),
            pl.BlockSpec((1, blocks, query_len), lambda h: (h, 0, 0)),
        ],
        out_specs=pl.BlockSpec((query_len, head_dim), lambda h: (0, h)),
        out_shape=jax.ShapeDtypeStruct((query_len, width), jnp.bfloat16),
        compiler_params=pltpu.CompilerParams(vmem_limit_bytes=40 * 1024 * 1024),
        cost_estimate=pl.CostEstimate(
            flops=pairs * 2 * (2 * head_dim + query_len),
            bytes_accessed=4 * length * width,
            transcendentals=3 * pairs,
        ),
        name="stick",
    )(place, queries, key_all, value_all, offset_all)


def routed_experts(rows, gain, gate_w, up_w, down_w, expert_ids, route_weights):
    ep_count = lax.axis_size("ep")
    tp_count = lax.axis_size("tp")
    local_experts = gate_w.shape[0]
    experts_all = ep_count * local_experts
    token_count = rows.shape[0]
    choose_count = expert_ids.shape[1]
    width = rows.shape[1]
    capacity = 2 * choose_count * token_count // experts_all
    part = capacity // tp_count
    rows_float = rows.astype(jnp.float32)
    normed = rows_float * lax.rsqrt(
        jnp.mean(rows_float * rows_float, axis=1, keepdims=True) + EPSILON
    )
    normed = (normed * gain[None, :]).astype(jnp.bfloat16)
    flat_ids = expert_ids.reshape(-1)
    onehot = (flat_ids[:, None] == jnp.arange(experts_all, dtype=jnp.int32)[None, :]).astype(
        jnp.int32
    )
    ranked = jnp.sum((jnp.cumsum(onehot, axis=0) - onehot) * onehot, axis=1)
    slot_index = flat_ids * capacity + ranked
    mine = lax.axis_index("tp") * part + jnp.arange(part, dtype=jnp.int32)
    wanted = (jnp.arange(experts_all, dtype=jnp.int32)[:, None] * capacity + mine).reshape(-1)
    pick = jnp.sum(
        (wanted[:, None, None] == slot_index.reshape(1, token_count, choose_count)), axis=2
    ).astype(jnp.bfloat16)
    outgoing = jnp.dot(pick, normed, preferred_element_type=jnp.float32).astype(jnp.bfloat16)
    outgoing = outgoing.reshape(ep_count, local_experts * part, width)
    arrived = lax.all_to_all(outgoing, "ep", split_axis=0, concat_axis=0, tiled=True)
    slots = lax.all_gather(arrived, "tp", axis=0)
    slots = slots.reshape(tp_count * ep_count, local_experts, part, width)
    slots = jnp.swapaxes(slots, 0, 1).reshape(local_experts, -1, width)
    gate_val = jnp.einsum("xnd,xdf->xnf", slots, gate_w, preferred_element_type=jnp.float32)
    up_val = jnp.einsum("xnd,xdf->xnf", slots, up_w, preferred_element_type=jnp.float32)
    hidden = (jax.nn.silu(gate_val) * up_val).astype(jnp.bfloat16)
    parts = jnp.einsum("xnf,xfd->xnd", hidden, down_w, preferred_element_type=jnp.float32).astype(
        jnp.bfloat16
    )
    share = lax.psum_scatter(parts, "tp", scatter_dimension=2, tiled=True)
    share = share.reshape(local_experts, tp_count, ep_count, part, width // tp_count)
    returned = lax.all_to_all(share, "ep", split_axis=2, concat_axis=0, tiled=True)
    flat_out = returned.reshape(experts_all * capacity, width // tp_count)
    picked = flat_out[slot_index].astype(jnp.float32)
    picked = picked.reshape(token_count, choose_count, width // tp_count)
    mixed = jnp.sum(picked * route_weights[:, :, None], axis=1).astype(jnp.bfloat16)
    return lax.all_gather(mixed, "tp", axis=1, tiled=True)


def body(
    queries, keys, values, key_offset, rows, gain, gate_w, up_w, down_w, expert_ids, route_weights
):
    attended = stick_mixer(queries, keys, values, key_offset)
    mixed = routed_experts(rows, gain, gate_w, up_w, down_w, expert_ids, route_weights)
    return (attended, mixed)


def solution(mesh):
    in_specs = (
        P("ep", "tp"),
        P("ep", "tp"),
        P("ep", "tp"),
        P("ep", "tp"),
        P("ep", None),
        P(),
        P("ep", None, "tp"),
        P("ep", None, "tp"),
        P("ep", "tp", None),
        P("ep", None),
        P("ep", None),
    )
    out_specs = (P("ep", "tp"), P("ep", None))
    return jax.shard_map(body, mesh=mesh, in_specs=in_specs, out_specs=out_specs, check_vma=False)
```

time: 678 us -> 253 us (0.37)
  local copies, waits for them, and re-layouts: 230 us -> 9.76 us
  other arithmetic: 155 us -> 2.88 us
  matrix products: 75.4 us -> 17.4 us
  blocking collectives: 109 us -> 67.9 us
  waiting for transfers between devices: 64.9 us -> 105 us
  Pallas kernels: 0 us -> 28.9 us
  loops' own time: 20.9 us -> 0 us
    dynamic_update_slice x24 -> x0, local copies, waits for them, and re-layouts: 183 us -> none  [stick_mixer(): lax.map(one_block, (key_split, value_split, offset_split, jnp.arange(bloc...]
    another operation x27 -> x2, other arithmetic: 118 us -> 0.62 us
    dot_general x20 -> x3, matrix products: 75.4 us -> 17.4 us  [the longest x1 9.57 us: routed_experts(): jnp.einsum('xnf,xfd->xnd', hidden, down_w, preferred_element_type=jnp.flo...]
    all_gather x3, waiting for transfers between devices: 32.6 us -> 74 us  [the longest x1 49.7 us: stick_mixer(): value_all = lax.all_gather(values, 'ep', axis=0, tiled=True)]
    all_to_all x1, blocking collectives: 51.5 us -> 17.7 us  [routed_experts(): lax.all_to_all(outgoing, 'ep', split_axis=0, concat_axis=0, tiled=True)]
    all_to_all x1 -> x0, blocking collectives: 32.5 us -> none  [routed_experts(): lax.all_to_all(share, 'ep', split_axis=1, concat_axis=1, tiled=True)]
    convert_element_type x10 -> x1, other arithmetic: 30.5 us -> 0.01 us  [stick_mixer(): offset_all = jnp.swapaxes(offset_all, 0, 1).astype(jnp.float32)]
    pallas_call x0 -> x1, Pallas kernels: none -> 28.9 us  [stick_mixer(): pl.pallas_call(stick_kernel, grid=(heads,), in_specs=[pl.BlockSpec(memory...]
  transfers between devices with their start and end apart: 4 -> 5, of which waited for: 2 -> 3; matrix products, arithmetic and copies ran while one was open for 63% -> 1% of each run, Pallas kernels for 0% -> 11%
where the time goes in v1:
time: 253 us
  waiting for transfers between devices  105 us (42%)
  blocking collectives  67.9 us (27%)
  Pallas kernels  28.9 us (11%)
  matrix products  17.4 us (7%)
  between operations  15.6 us (6%)
  local copies, waits for them, and re-layouts  9.76 us (4%)
  starting transfers between devices  5.6 us (2%)
  other arithmetic  2.88 us (1%)
    all_gather x1, waiting for transfers between devices, stick_mixer(): value_all = lax.all_gather(values, 'ep', axis=0, tiled=True)  49.7 us
    all_gather x1, blocking collectives, stick_mixer(): offset_all = lax.all_gather(key_offset.T, 'ep', axis=0)  42.4 us
    reduce_scatter x1, waiting for transfers between devices, routed_experts(): share = lax.psum_scatter(parts, 'tp', scatter_dimension=2, tiled=True)  29.5 us
    pallas_call x1, Pallas kernels, stick_mixer(): pl.pallas_call(stick_kernel, grid=(heads,), in_specs=[pl.BlockSpec(memory...  28.9 us
    all_gather x1, waiting for transfers between devices, routed_experts(): slots = lax.all_gather(arrived, 'tp', axis=0)  24.4 us
    all_to_all x1, blocking collectives, routed_experts(): lax.all_to_all(outgoing, 'ep', split_axis=0, concat_axis=0, tiled=True)  17.7 us
    dot_general x1, matrix products, routed_experts(): jnp.einsum('xnf,xfd->xnd', hidden, down_w, preferred_element_type=jnp.flo...  9.57 us
    all_gather x1, blocking collectives, routed_experts(): return lax.all_gather(mixed, 'tp', axis=1, tiled=True)  7.82 us
  transfers between devices with their start and end apart: 5, of which 3 were waited for; matrix products, arithmetic and copies ran while one was open for 1% of the time, Pallas kernels for 11%

profile of v1, /device:TPU:27, one launch (start us, length us, event | category | flops | bytes accessed | tf_op | source)
XLA Modules:
  0.0 252.6 jit_solution(17402201046894034655)
XLA Ops:
  8.0 0.0 all-gather.11.cloned.1.call-start
  8.0 0.8 copy.29
  8.8 0.1 eq.43
  9.0 0.1 eq.39
  9.1 1.2 fusion.14
  10.4 0.6 reduce-window.6
  11.0 0.2 slice_reduce_fusion
  11.2 0.1 fusion.24
  11.3 0.1 reduce_sum.41
  11.5 0.1 copy.32
  11.5 0.1 broadcast_add_fusion
  11.6 0.1 add.80
  11.7 0.1 convert_reduce_fusion
  11.8 1.4 convolution_convert_fusion
  13.2 17.7 %all_to_all.20 = bf16[8,16,2048]{2,1,0:T(8,128)(2,1)} all-to-all(bf16[8,16,2048]{2,1,0:T(8,128)(2,1)S(1)} %bitcast.46), channel_id=1, replica_groups=mesh['ep'=8,'tp'=4] {'ep'}, dimensions={0} | all-to-all | bytes 1048576 | tf_op jit(solution)/shard_map/all_to_all | solution.py:111
  30.9 0.0 all-gather.11.cloned.1.call-update
  30.9 0.0 reduce-scatter.2.cloned.1.call-start
  31.0 24.4 %all-gather.11.cloned.1.call-done = bf16[32,16,2048]{2,1,0:T(8,128)(2,1)} async-done(((bf16[8,16,2048]{2,1,0:T(8,128)(2,1)}), bf16[32,16,2048]{2,1,0:T(8,128)(2,1)}) %all-gather.11.cloned.1.call-update) | async-done | bytes 2097168 | tf_op jit(solution)/shard_map/all_gather | solution.py:112
  55.4 0.0 copy-start.5
  55.4 6.4 %fusion.4 = f32[512,896]{1,0:T(8,128)} fusion(bf16[512,2048]{1,0:T(8,128)(2,1)} %bitcast.51, bf16[1,2048,896]{2,1,0:T(8,128)(2,1)} %param.17), kind=kOutput, calls=%fused_computation.5 | convolution fusion | flops 1879048192 | bytes 7602176 | tf_op jit(solution)/shard_map/xnd,xdf->xnf/dot_general | solution.py:115
  61.8 0.0 copy-done.5
  61.8 9.6 %fusion.9 = bf16[1,512,2048]{2,1,0:T(8,128)(2,1)} fusion(bf16[1,896,2048]{2,1,0:T(8,128)(2,1)} %param.19, f32[512,896]{1,0:T(8,128)} %fusion.4, bf16[512,2048]{1,0:T(8,128)(2,1)S(1)} %bitcast.52, bf16[1,2048,896]{2,1,0:T(8,128)(2,1)} %param.18), kind=kOutput, calls=%fused_computation.8 | convolution fusion | flops 3761897472 | bytes 13369344 | tf_op jit(solution)/shard_map/xnf,xfd->xnd/dot_general | solution.py:118
  71.3 0.0 copy-start.4
  71.3 0.0 reduce-scatter.2.cloned.1.call-update
  71.4 0.0 all-gather.7.cloned.1.call-start
  71.4 0.5 all-gather.7.cloned.1.call-update
  71.9 0.0 all-gather.9.cloned.1.call-start
  72.0 0.5 all-gather.9.cloned.1.call-update
  72.5 0.1 mul.80
  72.7 29.5 %reduce-scatter.2.cloned.1.call-done = bf16[1,512,512]{2,1,0:T(8,128)(2,1)} async-done(((bf16[1,512,2048]{2,1,0:T(8,128)(2,1)}), bf16[1,512,512]{2,1,0:T(8,128)(2,1)}) %reduce-scatter.2.cloned.1.call-update) | async-done | bytes 524304 | tf_op jit(solution)/shard_map/reduce_scatter | solution.py:121
  102.1 1.9 copy.33
  104.0 5.4 %all-to-all-start.1 = ((bf16[1,4,8,16,512]{4,3,1,0,2:T(8,128)(2,1)}), bf16[1,4,8,16,512]{4,3,1,0,2:T(8,128)(2,1)S(1)}, u32[]{:S(2)}, u32[]{:S(2)}) async-start(bf16[1,4,8,16,512]{4,3,1,0,2:T(8,128)(2,1)} %copy.33), calls=%async_computation.2 | async-start | bytes 1048576 | tf_op jit(solution)/shard_map/all_to_all | solution.py:123
  109.5 0.0 copy-done.4
  109.5 0.1 copy.34
  109.6 0.0 copy-done.3
  109.6 42.4 %all-gather.2 = bf16[8,4,384]{2,1,0:T(4,128)(2,1)S(1)} all-gather(bf16[1,4,384]{2,1,0:T(4,128)(2,1)S(1)} %bitcast.50), channel_id=2, replica_groups=mesh['ep'=8,'tp'=4] {'ep'}, dimensions={0}, use_global_device_ids=true | all-gather | bytes 27648 | tf_op jit(solution)/shard_map/all_gather | solution.py:55
  152.0 0.0 all-gather.7.cloned.1.call-done.k_ref
  152.0 49.7 %all-gather.9.cloned.1.call-done.v_ref = bf16[3072,512]{1,0:T(8,128)(2,1)} async-done(((bf16[384,512]{1,0:T(8,128)(2,1)}), bf16[3072,512]{1,0:T(8,128)(2,1)}) %all-gather.9.cloned.1.call-update) | async-done | bytes 3145744 | tf_op jit(solution)/shard_map/all_gather | solution.py:54
  201.6 0.0 copy-done.2
  201.7 1.9 copy-done
  203.5 1.9 copy-done.1
  205.4 28.9 %stick.1 = bf16[384,512]{1,0:T(8,128)(2,1)} custom-call(s32[1]{0:T(128)} %bitcast.place_ref, bf16[384,512]{1,0:T(8,128)(2,1)S(1)} %copy-done.2, bf16[3072,512]{1,0:T(8,128)(2,1)S(1)} %copy-done, bf16[3072,512]{1,0:T(8,128)(2,1)S(1)} %copy-done.1, f32[4,8,384]{2,1,0:T(8,128)S(1)} %convert_bitcast_fusion.offset_ref), custom_call_target="tpu_custom_call" | custom-call | flops 6039797760 | bytes 6291456 | tf_op jit(solution)/shard_map/stick/pallas_call | solution.py:61
  234.3 0.0 all-to-all-done.1
  234.3 1.2 gather_fusion
  235.5 0.3 reshape.144
  235.8 0.7 multiply_reduce_fusion
  236.5 7.8 %all_gather.27 = bf16[128,2048]{1,0:T(8,128)(2,1)S(1)} all-gather(bf16[128,512]{1,0:T(8,128)(2,1)S(1)} %multiply_reduce_fusion), channel_id=1, replica_groups=mesh['ep'=8,'tp'=4] {'tp'}, dimensions={1}, use_global_device_ids=true | all-gather | bytes 655360 | tf_op jit(solution)/shard_map/all_gather | solution.py:128
  244.4 0.8 copy.37
  (14 shorter events, 0.1 us)
Async XLA Ops:
  8.0 47.4 %all-gather.11.cloned.1.call-start = ((), (), s32[]{:S(2)}) async-start(), calls=%async_computation.6 | async-start | bytes 2621440 | tf_op jit(solution)/shard_map/all_gather | solution.py:112
  30.9 71.2 %reduce-scatter.2.cloned.1.call-start = ((), (), s32[]{:S(2)}) async-start(), calls=%async_computation.5 | async-start | bytes 2621440 | tf_op jit(solution)/shard_map/reduce_scatter | solution.py:121
  55.4 6.4 %copy-start.5 = (bf16[32,16,2048]{2,1,0:T(8,128)(2,1)S(1)}, bf16[32,16,2048]{2,1,0:T(8,128)(2,1)}, u32[]{:S(2)}) copy-start(bf16[32,16,2048]{2,1,0:T(8,128)(2,1)} %all-gather.11.cloned.1.call-done) | copy-start | bytes 6291460
  71.3 38.1 %copy-start.4 = (f32[128,2]{0,1:T(2,128)S(1)}, f32[128,2]{0,1:T(2,128)}, u32[]{:S(2)}) copy-start(f32[128,2]{0,1:T(2,128)} %param.21) | copy-start | bytes 3076
  71.3 38.2 %copy-start.3 = (bf16[384,4]{0,1:T(4,128)(2,1)S(1)}, bf16[384,4]{0,1:T(4,128)(2,1)}, u32[]{:S(2)}) copy-start(bf16[384,4]{0,1:T(4,128)(2,1)} %param.14) | copy-start | bytes 9220
  71.3 130.3 %copy-start.2 = (bf16[384,512]{1,0:T(8,128)(2,1)S(1)}, bf16[384,512]{1,0:T(8,128)(2,1)}, u32[]{:S(2)}) copy-start(bf16[384,512]{1,0:T(8,128)(2,1)} %q_ref.1) | copy-start | bytes 1179652
  71.4 80.6 %all-gather.7.cloned.1.call-start = ((), (), s32[]{:S(2)}) async-start(), calls=%async_computation.3 | async-start | bytes 3538944 | tf_op jit(solution)/shard_map/all_gather | solution.py:53
  71.9 129.7 %all-gather.9.cloned.1.call-start = ((), (), s32[]{:S(2)}) async-start(), calls=%async_computation.4 | async-start | bytes 3538944 | tf_op jit(solution)/shard_map/all_gather | solution.py:54
  104.0 130.3 %all-to-all-start.1 = ((bf16[1,4,8,16,512]{4,3,1,0,2:T(8,128)(2,1)}), bf16[1,4,8,16,512]{4,3,1,0,2:T(8,128)(2,1)S(1)}, u32[]{:S(2)}, u32[]{:S(2)}) async-start(bf16[1,4,8,16,512]{4,3,1,0,2:T(8,128)(2,1)} %copy.33), calls=%async_computation.2 | async-start | bytes 1048576 | tf_op jit(solution)/shard_map/all_to_all | solution.py:123
  201.6 1.9 copy-start
  203.5 1.9 copy-start.1
Sparse Core Ops, SparseCore 0:
  31.1 24.2 all-gather.10
  71.5 30.6 reduce-scatter.1
Sparse Core Ops, SparseCore 1:
  74.0 67.2 all-gather.6
  143.4 58.2 all-gather.8

commit v2 on v1

--- a/solution.py
+++ b/solution.py
@@ -8,17 +8,18 @@
 EPSILON = 1e-06
 
 
-def stick_kernel(place_ref, q_ref, k_ref, v_ref, offset_ref, out_ref):
+def stick_kernel(
+    place_ref, q_ref, other_ref, k_ref, v_ref, offset_ref, total_ref, decay_ref, partial_ref
+):
     rows, head_dim = q_ref.shape
     scale = head_dim ** (-0.5)
-    place = place_ref[0]
+    place, others = place_ref[0], place_ref[1]
     across = lax.broadcasted_iota(jnp.int32, (rows, rows), 0)
     along = lax.broadcasted_iota(jnp.int32, (rows, rows), 1)
     strict = along < across
     after = jnp.where(strict, 1.0, 0.0).astype(jnp.bfloat16)
-    query = q_ref[...]
 
-    def one_block(block, masked):
+    def one_block(query, block, masked):
         here = pl.ds(pl.multiple_of(block * rows, rows), rows)
         logits = lax.dot_general(
             query, k_ref[here, :], (((1,), (1,)), ((), ())), preferred_element_type=jnp.float32
@@ -37,39 +38,60 @@
         )
         return summed, jnp.sum(breaks, axis=1, keepdims=True)
 
-    def step(index, carry):
-        total, later = carry
-        summed, block_total = one_block(place - 1 - index, False)
-        return total + jnp.exp(later) * summed, later + block_total
+    def walk(query, count, start):
+        def step(index, carry):
+            total, later = carry
+            summed, block_total = one_block(query, count - 1 - index, False)
+            return total + jnp.exp(later) * summed, later + block_total
 
-    total, _ = lax.fori_loop(0, place, step, one_block(place, True))
-    out_ref[...] = total.astype(out_ref.dtype)
+        return lax.fori_loop(0, count, step, start)
+
+    query = q_ref[...]
+    total, later = walk(query, place, one_block(query, place, True))
+    total_ref[...] = total
+    decay_ref[...] = jnp.broadcast_to(jnp.exp(later), total.shape)
+    nothing = (jnp.zeros((rows, head_dim), jnp.float32), jnp.zeros((rows, 1), jnp.float32))
+    partial, _ = walk(other_ref[...], others, nothing)
+    partial_ref[...] = partial.astype(partial_ref.dtype)
 
 
-def stick_mixer(queries, keys, values, key_offset):
+def halves():
+    count = lax.axis_size("ep")
+    half = count // 2
+    return half, [list(range(half)), list(range(half, count))]
+
+
+def gather_half(array, axis, tiled):
+    return lax.all_gather(array, "ep", axis=axis, tiled=tiled, axis_index_groups=halves()[1])
+
+
+def attend(queries, others, key_half, value_half, offset_half):
     query_len, width = queries.shape
-    heads = key_offset.shape[1]
+    heads, blocks = offset_half.shape[:2]
     head_dim = width // heads
-    key_all = lax.all_gather(keys, "ep", axis=0, tiled=True)
-    value_all = lax.all_gather(values, "ep", axis=0, tiled=True)
-    offset_all = lax.all_gather(key_offset.T, "ep", axis=0)
-    offset_all = jnp.swapaxes(offset_all, 0, 1).astype(jnp.float32)
-    blocks = offset_all.shape[1]
     length = blocks * query_len
-    place = lax.axis_index("ep").astype(jnp.int32).reshape(1)
-    pairs = heads * blocks * query_len * query_len
+    position = lax.axis_index("ep").astype(jnp.int32)
+    place = jnp.stack([position % blocks, jnp.where(position < blocks, blocks, 0)])
+    pairs = 2 * heads * blocks * query_len * query_len
+    one = pl.BlockSpec((query_len, head_dim), lambda h: (0, h))
+    whole = pl.BlockSpec((length, head_dim), lambda h: (0, h))
     return pl.pallas_call(
         stick_kernel,
         grid=(heads,),
         in_specs=[
             pl.BlockSpec(memory_space=pltpu.SMEM),
-            pl.BlockSpec((query_len, head_dim), lambda h: (0, h)),
-            pl.BlockSpec((length, head_dim), lambda h: (0, h)),
-            pl.BlockSpec((length, head_dim), lambda h: (0, h)),
+            one,
+            one,
+            whole,
+            whole,
             pl.BlockSpec((1, blocks, query_len), lambda h: (h, 0, 0)),
         ],
-        out_specs=pl.BlockSpec((query_len, head_dim), lambda h: (0, h)),
-        out_shape=jax.ShapeDtypeStruct((query_len, width), jnp.bfloat16),
+        out_specs=[one, one, one],
+        out_shape=[
+            jax.ShapeDtypeStruct((query_len, width), jnp.float32),
+            jax.ShapeDtypeStruct((query_len, width), jnp.float32),
+            jax.ShapeDtypeStruct((query_len, width), jnp.bfloat16),
+        ],
         compiler_params=pltpu.CompilerParams(vmem_limit_bytes=40 * 1024 * 1024),
         cost_estimate=pl.CostEstimate(
             flops=pairs * 2 * (2 * head_dim + query_len),
@@ -77,10 +99,18 @@
             transcendentals=3 * pairs,
         ),
         name="stick",
-    )(place, queries, key_all, value_all, offset_all)
+    )(place, queries, others, key_half, value_half, offset_half)
 
 
-def routed_experts(rows, gain, gate_w, up_w, down_w, expert_ids, route_weights):
+def layer(
+    queries, keys, values, key_offset, rows, gain, gate_w, up_w, down_w, expert_ids, route_weights
+):
+    half = halves()[0]
+    offset_half = gather_half(key_offset.T, 0, False)
+    rows, offset_half = lax.optimization_barrier((rows, offset_half))
+    offset_half = jnp.swapaxes(offset_half, 0, 1).astype(jnp.float32)
+    value_half = gather_half(values, 0, True)
+    others = lax.ppermute(queries, "ep", [(half + i, i) for i in range(half)])
     ep_count = lax.axis_size("ep")
     tp_count = lax.axis_size("tp")
     local_experts = gate_w.shape[0]
@@ -109,7 +139,10 @@
     outgoing = jnp.dot(pick, normed, preferred_element_type=jnp.float32).astype(jnp.bfloat16)
     outgoing = outgoing.reshape(ep_count, local_experts * part, width)
     arrived = lax.all_to_all(outgoing, "ep", split_axis=0, concat_axis=0, tiled=True)
+    arrived, value_half, others = lax.optimization_barrier((arrived, value_half, others))
     slots = lax.all_gather(arrived, "tp", axis=0)
+    slots, keys = lax.optimization_barrier((slots, keys))
+    key_half = gather_half(keys, 0, True)
     slots = slots.reshape(tp_count * ep_count, local_experts, part, width)
     slots = jnp.swapaxes(slots, 0, 1).reshape(local_experts, -1, width)
     gate_val = jnp.einsum("xnd,xdf->xnf", slots, gate_w, preferred_element_type=jnp.float32)
@@ -118,22 +151,19 @@
     parts = jnp.einsum("xnf,xfd->xnd", hidden, down_w, preferred_element_type=jnp.float32).astype(
         jnp.bfloat16
     )
+    parts, key_half, value_half = lax.optimization_barrier((parts, key_half, value_half))
+    total, decay, partial = attend(queries, others, key_half, value_half, offset_half)
     share = lax.psum_scatter(parts, "tp", scatter_dimension=2, tiled=True)
+    share, partial = lax.optimization_barrier((share, partial))
+    early = lax.ppermute(partial, "ep", [(i, half + i) for i in range(half)])
+    attended = (total + decay * early.astype(jnp.float32)).astype(jnp.bfloat16)
     share = share.reshape(local_experts, tp_count, ep_count, part, width // tp_count)
     returned = lax.all_to_all(share, "ep", split_axis=2, concat_axis=0, tiled=True)
     flat_out = returned.reshape(experts_all * capacity, width // tp_count)
     picked = flat_out[slot_index].astype(jnp.float32)
     picked = picked.reshape(token_count, choose_count, width // tp_count)
     mixed = jnp.sum(picked * route_weights[:, :, None], axis=1).astype(jnp.bfloat16)
-    return lax.all_gather(mixed, "tp", axis=1, tiled=True)
-
-
-def body(
-    queries, keys, values, key_offset, rows, gain, gate_w, up_w, down_w, expert_ids, route_weights
-):
-    attended = stick_mixer(queries, keys, values, key_offset)
-    mixed = routed_experts(rows, gain, gate_w, up_w, down_w, expert_ids, route_weights)
-    return (attended, mixed)
+    return attended, lax.all_gather(mixed, "tp", axis=1, tiled=True)
 
 
 def solution(mesh):
@@ -151,4 +181,4 @@
         P("ep", None),
     )
     out_specs = (P("ep", "tp"), P("ep", None))
-    return jax.shard_map(body, mesh=mesh, in_specs=in_specs, out_specs=out_specs, check_vma=False)
+    return jax.shard_map(layer, mesh=mesh, in_specs=in_specs, out_specs=out_specs, check_vma=False)

time: 253 us -> 208 us (0.82)
  blocking collectives: 67.9 us -> 15.7 us
  Pallas kernels: 28.9 us -> 15.3 us
  waiting for transfers between devices: 105 us -> 115 us
  starting transfers between devices: 5.6 us -> 14.5 us
    ppermute x0 -> x2, waiting for transfers between devices: none -> 43.6 us  [the longest x1 28.1 us: layer(): early = lax.ppermute(partial, 'ep', [(i, half + i) for i in range(half)])]
    all_gather x2, blocking collectives: 50.2 us -> 15.7 us  [the longest x1 8.47 us: gather_half(): lax.all_gather(array, 'ep', axis=axis, tiled=tiled, axis_index_groups=hal...]
    all_gather x3, waiting for transfers between devices: 74 us -> 54.8 us  [the longest x1 32 us: layer(): slots = lax.all_gather(arrived, 'tp', axis=0)]
    all_to_all x1 -> x0, blocking collectives: 17.7 us -> none  [routed_experts(): lax.all_to_all(outgoing, 'ep', split_axis=0, concat_axis=0, tiled=True)]
    reduce_scatter x1, waiting for transfers between devices: 29.5 us -> 15.8 us  [layer(): share = lax.psum_scatter(parts, 'tp', scatter_dimension=2, tiled=True)]
    pallas_call x1, Pallas kernels: 28.9 us -> 15.3 us  [attend(): pl.pallas_call(stick_kernel, grid=(heads,), in_specs=[pl.BlockSpec(memory...]
    all_to_all x1 -> x2, starting transfers between devices: 5.44 us -> 10.9 us  [the longest x1 5.44 us: layer(): lax.all_to_all(outgoing, 'ep', split_axis=0, concat_axis=0, tiled=True)]
    ppermute x0 -> x2, starting transfers between devices: none -> 3.49 us  [the longest x1 2.21 us: layer(): others = lax.ppermute(queries, 'ep', [(half + i, i) for i in range(half)])]
  transfers between devices with their start and end apart: 5 -> 8, of which waited for: 3 -> 6; matrix products, arithmetic and copies ran while one was open for 1% -> 12% of each run, Pallas kernels for 11% -> 7%
where the time goes in v2:
time: 208 us; the launch traced here: 207 us
  waiting for transfers between devices  115 us (55%)
  matrix products  18.6 us (9%)
  blocking collectives  15.7 us (8%)
  Pallas kernels  15.3 us (7%)
  starting transfers between devices  14.5 us (7%)
  between operations  13.9 us (7%)
  local copies, waits for them, and re-layouts  9.93 us (5%)
  other arithmetic  4.55 us (2%)
    all_gather x1, waiting for transfers between devices, layer(): slots = lax.all_gather(arrived, 'tp', axis=0)  32 us
    ppermute x1, waiting for transfers between devices, layer(): early = lax.ppermute(partial, 'ep', [(i, half + i) for i in range(half)])  28.1 us
    all_gather x2, waiting for transfers between devices, gather_half(): lax.all_gather(array, 'ep', axis=axis, tiled=tiled, axis_index_groups=hal...  22.8 us
    reduce_scatter x1, waiting for transfers between devices, layer(): share = lax.psum_scatter(parts, 'tp', scatter_dimension=2, tiled=True)  15.8 us
    ppermute x1, waiting for transfers between devices, layer(): others = lax.ppermute(queries, 'ep', [(half + i, i) for i in range(half)])  15.6 us
    pallas_call x1, Pallas kernels, attend(): pl.pallas_call(stick_kernel, grid=(heads,), in_specs=[pl.BlockSpec(memory...  15.3 us
    dot_general x1, matrix products, layer(): jnp.einsum('xnf,xfd->xnd', hidden, down_w, preferred_element_type=jnp.flo...  9.97 us
    all_gather x1, blocking collectives, gather_half(): lax.all_gather(array, 'ep', axis=axis, tiled=tiled, axis_index_groups=hal...  8.47 us
  transfers between devices with their start and end apart: 8, of which 6 were waited for; matrix products, arithmetic and copies ran while one was open for 12% of the time, Pallas kernels for 7%

profile of v2, /device:TPU:27, one launch (start us, length us, event | category | flops | bytes accessed | tf_op | source)
XLA Modules:
  0.0 207.5 jit_solution(15772274774037474041)
XLA Ops:
  7.2 0.0 all-gather.7.cloned.1.call-start
  7.2 0.7 all-gather.7.cloned.1.call-update
  7.9 0.8 copy.28
  8.7 0.1 eq.45
  8.8 0.1 eq.41
  9.0 0.6 reduce-window.6
  9.6 0.2 slice_reduce_fusion
  9.8 0.1 fusion.24
  9.9 0.1 reduce_sum.41
  10.1 0.6 broadcast_multiply_fusion
  10.7 0.1 copy.31
  10.8 0.1 broadcast_add_fusion
  10.9 0.1 add.88
  10.9 8.5 %all-gather.2 = bf16[4,4,384]{2,1,0:T(4,128)(2,1)S(1)} all-gather(bf16[1,4,384]{2,1,0:T(4,128)(2,1)} %bitcast.51), channel_id=2, replica_groups={{0,4,8,12},{16,20,24,28},{1,5,9,13},{17,21,25,29},{2,6,10,14},{18,22,26..., dimensions={0}, use_global_device_ids=true | all-gather | bytes 15360 | tf_op jit(solution)/shard_map/all_gather | solution.py:65
  19.4 0.1 convert_reduce_fusion
  19.5 1.2 fusion.14
  20.7 2.2 %convolution_convert_fusion = bf16[128,2048]{1,0:T(8,128)(2,1)} fusion(bf16[128,2048]{1,0:T(8,128)(2,1)} %param.15, f32[2048]{0:T(1024)} %param.16, f32[128]{0:T(128)S(1)} %add_rsqrt_fusion, s32[128,128]{1,0:T(8,128)S(1)} %convert_reduce_fusion), kind=kOutput, calls=%fused_computation.9 | convolution fusion | flops 68435968 | bytes 1122816 | tf_op jit(solution)/shard_map/dot_general | solution.py:139
  23.0 5.4 %all-to-all-start = ((bf16[8,16,2048]{2,1,0:T(8,128)(2,1)}), bf16[8,16,2048]{2,1,0:T(8,128)(2,1)S(1)}, u32[]{:S(2)}, u32[]{:S(2)}) async-start(bf16[8,16,2048]{2,1,0:T(8,128)(2,1)} %bitcast.6), calls=%async_computation | async-start | bytes 1048576 | tf_op jit(solution)/shard_map/all_to_all | solution.py:141
  28.4 2.2 %collective-permute-start = (bf16[384,512]{1,0:T(8,128)(2,1)S(1)}, bf16[384,512]{1,0:T(8,128)(2,1)S(1)}, u32[]{:S(2)}, u32[]{:S(2)}) collective-permute-start(bf16[384,512]{1,0:T(8,128)(2,1)S(1)} %copy-done.2), channel_id=1, source_target_pairs={{16,0},{20,4},{24,8},{28,12},{17,1},{21,5},{25,9},{29,13},{18,2},{... | collective-permute-start | bytes 1179656 | tf_op jit(solution)/shard_map/ppermute | solution.py:113
  30.6 15.6 %collective-permute-done.other_ref = bf16[384,512]{1,0:T(8,128)(2,1)S(1)} collective-permute-done((bf16[384,512]{1,0:T(8,128)(2,1)S(1)}, bf16[384,512]{1,0:T(8,128)(2,1)S(1)}, u32[]{:S(2)}, u32[]{:S(2)}) %collective-permute-start) | collective-permute-done | bytes 393248 | tf_op jit(solution)/shard_map/ppermute | solution.py:113
  46.2 0.7 copy-done.3
  47.0 3.6 %all-gather.7.cloned.1.call-done.v_ref = bf16[1536,512]{1,0:T(8,128)(2,1)} async-done(((bf16[384,512]{1,0:T(8,128)(2,1)}), bf16[1536,512]{1,0:T(8,128)(2,1)}) %all-gather.7.cloned.1.call-update) | async-done | bytes 1572880 | tf_op jit(solution)/shard_map/all_gather | solution.py:65
  50.6 0.0 all-gather.11.cloned.1.call-update
  50.6 0.0 all-gather.9.cloned.1.call-start
  50.7 32.0 %all-gather.11.cloned.1.call-done = bf16[32,16,2048]{2,1,0:T(8,128)(2,1)} async-done(((bf16[8,16,2048]{2,1,0:T(8,128)(2,1)}), bf16[32,16,2048]{2,1,0:T(8,128)(2,1)}) %all-gather.11.cloned.1.call-update) | async-done | bytes 2097168 | tf_op jit(solution)/shard_map/all_gather | solution.py:143
  82.7 0.0 all-gather.9.cloned.1.call-update
  82.7 0.0 reduce-scatter.2.cloned.1.call-start
  82.8 6.4 %fusion.4 = f32[512,896]{1,0:T(8,128)} fusion(bf16[512,2048]{1,0:T(8,128)(2,1)} %bitcast.52, bf16[1,2048,896]{2,1,0:T(8,128)(2,1)} %param.17), kind=kOutput, calls=%fused_computation.5 | convolution fusion | flops 1879048192 | bytes 7602176 | tf_op jit(solution)/shard_map/xnd,xdf->xnf/dot_general | solution.py:148
  89.1 10.0 %fusion.9 = bf16[1,512,2048]{2,1,0:T(8,128)(2,1)} fusion(bf16[1,896,2048]{2,1,0:T(8,128)(2,1)} %param.19, f32[512,896]{1,0:T(8,128)} %fusion.4, bf16[512,2048]{1,0:T(8,128)(2,1)S(1)} %bitcast.53, bf16[1,2048,896]{2,1,0:T(8,128)(2,1)} %param.18), kind=kOutput, calls=%fused_computation.8 | convolution fusion | flops 3761897472 | bytes 13369344 | tf_op jit(solution)/shard_map/xnf,xfd->xnd/dot_general | solution.py:151
  99.1 19.2 %all-gather.9.cloned.1.call-done.k_ref = bf16[1536,512]{1,0:T(8,128)(2,1)} async-done(((bf16[384,512]{1,0:T(8,128)(2,1)}), bf16[1536,512]{1,0:T(8,128)(2,1)}) %all-gather.9.cloned.1.call-update) | async-done | bytes 1572880 | tf_op jit(solution)/shard_map/all_gather | solution.py:65
  118.3 0.1 pad_add_fusion.place_ref
  118.4 1.4 copy-done.1
  119.8 1.0 copy-done.4
  120.8 15.3 %stick.1 = (f32[384,512]{1,0:T(8,128)S(1)}, f32[384,512]{1,0:T(8,128)S(1)}, bf16[384,512]{1,0:T(8,128)(2,1)S(1)}) custom-call(s32[2]{0:T(128)S(1)} %pad_add_fusion.place_ref, bf16[384,512]{1,0:T(8,128)(2,1)S(1)} %copy-done.2, bf16[384,512]{1,0:T(8,128)(2,1)S(1)} %copy-done.4, bf16[1536,512]{1,0:T(8,128)(2,1)S(1)} %copy-done.1, ...), custom_call_target="tpu_custom_call" | custom-call | flops 6039797760 | bytes 3145728 | tf_op jit(solution)/shard_map/stick/pallas_call | solution.py:78
  136.1 0.7 copy-done.5
  136.8 15.8 %reduce-scatter.2.cloned.1.call-done = bf16[1,512,512]{2,1,0:T(8,128)(2,1)} async-done(((bf16[1,512,2048]{2,1,0:T(8,128)(2,1)}), bf16[1,512,512]{2,1,0:T(8,128)(2,1)}) %reduce-scatter.2.cloned.1.call-update) | async-done | bytes 524304 | tf_op jit(solution)/shard_map/reduce_scatter | solution.py:156
  152.6 1.9 copy.33
  154.6 5.4 %all-to-all-start.1 = ((bf16[1,4,8,16,512]{4,3,1,0,2:T(8,128)(2,1)}), bf16[1,4,8,16,512]{4,3,1,0,2:T(8,128)(2,1)S(1)}, u32[]{:S(2)}, u32[]{:S(2)}) async-start(bf16[1,4,8,16,512]{4,3,1,0,2:T(8,128)(2,1)} %copy.33), calls=%async_computation.2 | async-start | bytes 1048576 | tf_op jit(solution)/shard_map/all_to_all | solution.py:161
  160.0 1.3 collective-permute-start.1
  161.3 0.1 mul.84
  161.5 0.1 copy.34
  161.6 28.1 %collective-permute-done.1 = bf16[384,512]{1,0:T(8,128)(2,1)S(1)} collective-permute-done((bf16[384,512]{1,0:T(8,128)(2,1)S(1)}, bf16[384,512]{1,0:T(8,128)(2,1)S(1)}, u32[]{:S(2)}, u32[]{:S(2)}) %collective-permute-start.1) | collective-permute-done | bytes 393248 | tf_op jit(solution)/shard_map/ppermute | solution.py:158
  189.6 1.0 add_convert_fusion
  190.6 1.2 gather_fusion
  191.8 0.3 reshape.140
  192.1 0.7 multiply_reduce_fusion
  192.9 7.3 %all_gather.27 = bf16[128,2048]{1,0:T(8,128)(2,1)S(1)} all-gather(bf16[128,512]{1,0:T(8,128)(2,1)S(1)} %multiply_reduce_fusion), channel_id=1, replica_groups=mesh['ep'=8,'tp'=4] {'tp'}, dimensions={1}, use_global_device_ids=true | all-gather | bytes 655360 | tf_op jit(solution)/shard_map/all_gather | solution.py:166
  200.1 0.8 copy.37
  (31 shorter events, 0.1 us)
Async XLA Ops:
  7.2 21.2 %copy-start.2 = (bf16[384,512]{1,0:T(8,128)(2,1)S(1)}, bf16[384,512]{1,0:T(8,128)(2,1)}, u32[]{:S(2)}) copy-start(bf16[384,512]{1,0:T(8,128)(2,1)} %q_ref.1) | copy-start | bytes 1179652
  7.2 43.4 %all-gather.7.cloned.1.call-start = ((), (), s32[]{:S(2)}) async-start(), calls=%async_computation.3 | async-start | bytes 1966080 | tf_op jit(solution)/shard_map/all_gather | solution.py:65
  23.0 24.0 %all-to-all-start = ((bf16[8,16,2048]{2,1,0:T(8,128)(2,1)}), bf16[8,16,2048]{2,1,0:T(8,128)(2,1)S(1)}, u32[]{:S(2)}, u32[]{:S(2)}) async-start(bf16[8,16,2048]{2,1,0:T(8,128)(2,1)} %bitcast.6), calls=%async_computation | async-start | bytes 1048576 | tf_op jit(solution)/shard_map/all_to_all | solution.py:141
  28.4 54.3 %all-gather.11.cloned.1.call-start = ((), (), s32[]{:S(2)}) async-start(), calls=%async_computation.6 | async-start | bytes 2621440 | tf_op jit(solution)/shard_map/all_gather | solution.py:143
  28.4 17.8 %collective-permute-start = (bf16[384,512]{1,0:T(8,128)(2,1)S(1)}, bf16[384,512]{1,0:T(8,128)(2,1)S(1)}, u32[]{:S(2)}, u32[]{:S(2)}) collective-permute-start(bf16[384,512]{1,0:T(8,128)(2,1)S(1)} %copy-done.2), channel_id=1, source_target_pairs={{16,0},{20,4},{24,8},{28,12},{17,1},{21,5},{25,9},{29,13},{18,2},{... | collective-permute-start | bytes 1179656 | tf_op jit(solution)/shard_map/ppermute | solution.py:113
  46.2 0.7 copy-start.3
  47.0 3.6 %copy-start.7 = (bf16[8,16,2048]{2,1,0:T(8,128)(2,1)}, bf16[8,16,2048]{2,1,0:T(8,128)(2,1)S(1)}, u32[]{:S(2)}) copy-start(bf16[8,16,2048]{2,1,0:T(8,128)(2,1)S(1)} %all-to-all-done) | copy-start | bytes 1572868
  50.6 67.6 %all-gather.9.cloned.1.call-start = ((), (), s32[]{:S(2)}) async-start(), calls=%async_computation.4 | async-start | bytes 1966080 | tf_op jit(solution)/shard_map/all_gather | solution.py:65
  82.7 69.9 %reduce-scatter.2.cloned.1.call-start = ((), (), s32[]{:S(2)}) async-start(), calls=%async_computation.5 | async-start | bytes 2621440 | tf_op jit(solution)/shard_map/reduce_scatter | solution.py:156
  82.7 6.4 %copy-start.10 = (bf16[32,16,2048]{2,1,0:T(8,128)(2,1)S(1)}, bf16[32,16,2048]{2,1,0:T(8,128)(2,1)}, u32[]{:S(2)}) copy-start(bf16[32,16,2048]{2,1,0:T(8,128)(2,1)} %all-gather.11.cloned.1.call-done) | copy-start | bytes 6291460
  99.1 19.3 %copy-start = (bf16[1536,512]{1,0:T(8,128)(2,1)S(1)}, bf16[1536,512]{1,0:T(8,128)(2,1)}, u32[]{:S(2)}) copy-start(bf16[1536,512]{1,0:T(8,128)(2,1)} %all-gather.7.cloned.1.call-done.v_ref) | copy-start | bytes 4718596
  118.4 1.4 copy-start.1
  119.8 1.0 copy-start.4
  136.1 0.7 copy-start.5
  136.8 24.5 %copy-start.8 = (s32[128,2]{1,0:T(8,128)S(1)}, s32[128,2]{1,0:T(8,128)}, u32[]{:S(2)}) copy-start(s32[128,2]{1,0:T(8,128)} %get-tuple-element.32) | copy-start | bytes 3076
  136.8 24.6 %copy-start.9 = (f32[128,2]{0,1:T(2,128)S(1)}, f32[128,2]{0,1:T(2,128)}, u32[]{:S(2)}) copy-start(f32[128,2]{0,1:T(2,128)} %param.21) | copy-start | bytes 3076
  152.6 7.4 %copy-start.6 = (bf16[384,512]{1,0:T(8,128)(2,1)S(1)}, bf16[384,512]{1,0:T(8,128)(2,1)}, u32[]{:S(2)}) copy-start(bf16[384,512]{1,0:T(8,128)(2,1)} %copy-done.5) | copy-start | bytes 1179652
  154.6 36.1 %all-to-all-start.1 = ((bf16[1,4,8,16,512]{4,3,1,0,2:T(8,128)(2,1)}), bf16[1,4,8,16,512]{4,3,1,0,2:T(8,128)(2,1)S(1)}, u32[]{:S(2)}, u32[]{:S(2)}) async-start(bf16[1,4,8,16,512]{4,3,1,0,2:T(8,128)(2,1)} %copy.33), calls=%async_computation.2 | async-start | bytes 1048576 | tf_op jit(solution)/shard_map/all_to_all | solution.py:161
  160.0 29.6 %collective-permute-start.1 = (bf16[384,512]{1,0:T(8,128)(2,1)S(1)}, bf16[384,512]{1,0:T(8,128)(2,1)S(1)}, u32[]{:S(2)}, u32[]{:S(2)}) collective-permute-start(bf16[384,512]{1,0:T(8,128)(2,1)S(1)} %copy-done.6), channel_id=1, source_target_pairs={{0,16},{4,20},{8,24},{12,28},{1,17},{5,21},{9,25},{13,29},{2,18},{... | collective-permute-start | bytes 1179656 | tf_op jit(solution)/shard_map/ppermute | solution.py:158
Sparse Core Ops, SparseCore 0:
  9.5 41.0 all-gather.6
  52.7 29.9 all-gather.10
  84.2 33.9 all-gather.8
  120.6 31.9 reduce-scatter.1

commit v3 on v2

--- a/solution.py
+++ b/solution.py
@@ -109,6 +109,7 @@
     offset_half = gather_half(key_offset.T, 0, False)
     rows, offset_half = lax.optimization_barrier((rows, offset_half))
     offset_half = jnp.swapaxes(offset_half, 0, 1).astype(jnp.float32)
+    key_half = gather_half(keys, 0, True)
     value_half = gather_half(values, 0, True)
     others = lax.ppermute(queries, "ep", [(half + i, i) for i in range(half)])
     ep_count = lax.axis_size("ep")
@@ -139,10 +140,13 @@
     outgoing = jnp.dot(pick, normed, preferred_element_type=jnp.float32).astype(jnp.bfloat16)
     outgoing = outgoing.reshape(ep_count, local_experts * part, width)
     arrived = lax.all_to_all(outgoing, "ep", split_axis=0, concat_axis=0, tiled=True)
-    arrived, value_half, others = lax.optimization_barrier((arrived, value_half, others))
+    arrived, key_half, value_half, others = lax.optimization_barrier(
+        (arrived, key_half, value_half, others)
+    )
     slots = lax.all_gather(arrived, "tp", axis=0)
-    slots, keys = lax.optimization_barrier((slots, keys))
-    key_half = gather_half(keys, 0, True)
+    total, decay, partial = attend(queries, others, key_half, value_half, offset_half)
+    slots, partial = lax.optimization_barrier((slots, partial))
+    early = lax.ppermute(partial, "ep", [(i, half + i) for i in range(half)])
     slots = slots.reshape(tp_count * ep_count, local_experts, part, width)
     slots = jnp.swapaxes(slots, 0, 1).reshape(local_experts, -1, width)
     gate_val = jnp.einsum("xnd,xdf->xnf", slots, gate_w, preferred_element_type=jnp.float32)
@@ -151,11 +155,8 @@
     parts = jnp.einsum("xnf,xfd->xnd", hidden, down_w, preferred_element_type=jnp.float32).astype(
         jnp.bfloat16
     )
-    parts, key_half, value_half = lax.optimization_barrier((parts, key_half, value_half))
-    total, decay, partial = attend(queries, others, key_half, value_half, offset_half)
     share = lax.psum_scatter(parts, "tp", scatter_dimension=2, tiled=True)
-    share, partial = lax.optimization_barrier((share, partial))
-    early = lax.ppermute(partial, "ep", [(i, half + i) for i in range(half)])
+    share, early = lax.optimization_barrier((share, early))
     attended = (total + decay * early.astype(jnp.float32)).astype(jnp.bfloat16)
     share = share.reshape(local_experts, tp_count, ep_count, part, width // tp_count)
     returned = lax.all_to_all(share, "ep", split_axis=2, concat_axis=0, tiled=True)

time: 208 us -> 207 us (level); the launches traced: 207 us -> 204 us
    all_gather x1, waiting for transfers between devices: 32 us -> 7.78 us  [layer(): slots = lax.all_gather(arrived, 'tp', axis=0)]
    all_gather x2, waiting for transfers between devices: 22.8 us -> 41.1 us  [gather_half(): lax.all_gather(array, 'ep', axis=axis, tiled=tiled, axis_index_groups=hal...]
    all_to_all x1, waiting for transfers between devices: 0.01 us -> 11.5 us  [layer(): lax.all_to_all(share, 'ep', split_axis=2, concat_axis=0, tiled=True)]
    ppermute x1, waiting for transfers between devices: 28.1 us -> 20.9 us  [layer(): early = lax.ppermute(partial, 'ep', [(i, half + i) for i in range(half)])]
    unnamed x25 -> x15, local copies, waits for them, and re-layouts: 5.6 us -> 4.53 us
  transfers between devices with their start and end apart: 8 -> 8, of which waited for: 6 -> 7; matrix products, arithmetic and copies ran while one was open for 12% -> 3% of each run, Pallas kernels for 7% -> 8%
where the time goes in v3:
time: 207 us; the launch traced here: 204 us
  waiting for transfers between devices  113 us (55%)
  matrix products  18.3 us (9%)
  blocking collectives  15.7 us (8%)
  Pallas kernels  15.3 us (7%)
  starting transfers between devices  14.5 us (7%)
  between operations  13.9 us (7%)
  local copies, waits for them, and re-layouts  8.8 us (4%)
  other arithmetic  3.92 us (2%)
    all_gather x2, waiting for transfers between devices, gather_half(): lax.all_gather(array, 'ep', axis=axis, tiled=tiled, axis_index_groups=hal...  41.1 us
    ppermute x1, waiting for transfers between devices, layer(): early = lax.ppermute(partial, 'ep', [(i, half + i) for i in range(half)])  20.9 us
    ppermute x1, waiting for transfers between devices, layer(): others = lax.ppermute(queries, 'ep', [(half + i, i) for i in range(half)])  16.3 us
    pallas_call x1, Pallas kernels, attend(): pl.pallas_call(stick_kernel, grid=(heads,), in_specs=[pl.BlockSpec(memory...  15.3 us
    reduce_scatter x1, waiting for transfers between devices, layer(): share = lax.psum_scatter(parts, 'tp', scatter_dimension=2, tiled=True)  14.2 us
    all_to_all x1, waiting for transfers between devices, layer(): lax.all_to_all(share, 'ep', split_axis=2, concat_axis=0, tiled=True)  11.5 us
    dot_general x1, matrix products, layer(): jnp.einsum('xnf,xfd->xnd', hidden, down_w, preferred_element_type=jnp.flo...  10.1 us
    all_gather x1, blocking collectives, gather_half(): lax.all_gather(array, 'ep', axis=axis, tiled=tiled, axis_index_groups=hal...  8.46 us
  transfers between devices with their start and end apart: 8, of which 7 were waited for; matrix products, arithmetic and copies ran while one was open for 3% of the time, Pallas kernels for 8%

profile of v3, /device:TPU:27, one launch (start us, length us, event | category | flops | bytes accessed | tf_op | source)
XLA Modules:
  0.0 203.7 jit_solution(15781684182516532295)
XLA Ops:
  7.2 0.0 copy-start.3
  7.2 0.0 all-gather.7.cloned.1.call-start
  7.2 0.7 all-gather.7.cloned.1.call-update
  7.9 0.0 all-gather.9.cloned.1.call-start
  8.0 0.7 all-gather.9.cloned.1.call-update
  8.7 0.8 copy.28
  9.5 0.1 eq.45
  9.6 0.1 eq.41
  9.7 0.6 reduce-window.6
  10.3 0.2 slice_reduce_fusion
  10.6 0.1 fusion.24
  10.7 8.5 %all-gather.2 = bf16[4,4,384]{2,1,0:T(4,128)(2,1)S(1)} all-gather(bf16[1,4,384]{2,1,0:T(4,128)(2,1)} %bitcast.51), channel_id=2, replica_groups={{0,4,8,12},{16,20,24,28},{1,5,9,13},{17,21,25,29},{2,6,10,14},{18,22,26..., dimensions={0}, use_global_device_ids=true | all-gather | bytes 15360 | tf_op jit(solution)/shard_map/all_gather | solution.py:65
  19.2 0.1 reduce_sum.41
  19.3 0.1 copy.31
  19.4 0.1 broadcast_add_fusion
  19.5 0.1 add.88
  19.6 0.1 convert_reduce_fusion
  19.7 1.2 fusion.14
  20.9 1.9 convolution_convert_fusion
  22.8 5.4 %all-to-all-start = ((bf16[8,16,2048]{2,1,0:T(8,128)(2,1)}), bf16[8,16,2048]{2,1,0:T(8,128)(2,1)S(1)}, u32[]{:S(2)}, u32[]{:S(2)}) async-start(bf16[8,16,2048]{2,1,0:T(8,128)(2,1)} %bitcast.6), calls=%async_computation | async-start | bytes 1048576 | tf_op jit(solution)/shard_map/all_to_all | solution.py:142
  28.2 2.2 %collective-permute-start = (bf16[384,512]{1,0:T(8,128)(2,1)S(1)}, bf16[384,512]{1,0:T(8,128)(2,1)S(1)}, u32[]{:S(2)}, u32[]{:S(2)}) collective-permute-start(bf16[384,512]{1,0:T(8,128)(2,1)S(1)} %copy-done.2), channel_id=1, source_target_pairs={{16,0},{20,4},{24,8},{28,12},{17,1},{21,5},{25,9},{29,13},{18,2},{... | collective-permute-start | bytes 1179656 | tf_op jit(solution)/shard_map/ppermute | solution.py:114
  30.5 16.3 %collective-permute-done.other_ref = bf16[384,512]{1,0:T(8,128)(2,1)S(1)} collective-permute-done((bf16[384,512]{1,0:T(8,128)(2,1)S(1)}, bf16[384,512]{1,0:T(8,128)(2,1)S(1)}, u32[]{:S(2)}, u32[]{:S(2)}) %collective-permute-start) | collective-permute-done | bytes 393248 | tf_op jit(solution)/shard_map/ppermute | solution.py:114
  46.8 3.8 %all-gather.7.cloned.1.call-done.k_ref = bf16[1536,512]{1,0:T(8,128)(2,1)} async-done(((bf16[384,512]{1,0:T(8,128)(2,1)}), bf16[1536,512]{1,0:T(8,128)(2,1)}) %all-gather.7.cloned.1.call-update) | async-done | bytes 1572880 | tf_op jit(solution)/shard_map/all_gather | solution.py:65
  50.6 37.2 %all-gather.9.cloned.1.call-done.v_ref = bf16[1536,512]{1,0:T(8,128)(2,1)} async-done(((bf16[384,512]{1,0:T(8,128)(2,1)}), bf16[1536,512]{1,0:T(8,128)(2,1)}) %all-gather.9.cloned.1.call-update) | async-done | bytes 1572880 | tf_op jit(solution)/shard_map/all_gather | solution.py:65
  87.8 0.0 all-gather.11.cloned.1.call-update
  87.9 0.0 reduce-scatter.2.cloned.1.call-start
  87.9 0.1 pad_add_fusion.place_ref
  88.0 1.4 copy-done
  89.4 1.4 copy-done.1
  90.8 15.3 %stick.1 = (f32[384,512]{1,0:T(8,128)S(1)}, f32[384,512]{1,0:T(8,128)S(1)}, bf16[384,512]{1,0:T(8,128)(2,1)S(1)}) custom-call(s32[2]{0:T(128)S(1)} %pad_add_fusion.place_ref, bf16[384,512]{1,0:T(8,128)(2,1)S(1)} %copy-done.2, bf16[384,512]{1,0:T(8,128)(2,1)S(1)} %collective-permute-done.other_ref, bf16[1536,512]{1,0:T(8,128)(2,1)S(1)} %copy-done, ...), custom_call_target="tpu_custom_call" | custom-call | flops 6039797760 | bytes 3145728 | tf_op jit(solution)/shard_map/stick/pallas_call | solution.py:78
  106.1 7.8 %all-gather.11.cloned.1.call-done = bf16[32,16,2048]{2,1,0:T(8,128)(2,1)} async-done(((bf16[8,16,2048]{2,1,0:T(8,128)(2,1)}), bf16[32,16,2048]{2,1,0:T(8,128)(2,1)}) %all-gather.11.cloned.1.call-update) | async-done | bytes 2097168 | tf_op jit(solution)/shard_map/all_gather | solution.py:146
  113.9 6.3 %fusion.4 = f32[512,896]{1,0:T(8,128)} fusion(bf16[512,2048]{1,0:T(8,128)(2,1)} %bitcast.52, bf16[1,2048,896]{2,1,0:T(8,128)(2,1)} %param.17), kind=kOutput, calls=%fused_computation.5 | convolution fusion | flops 1879048192 | bytes 7602176 | tf_op jit(solution)/shard_map/xnd,xdf->xnf/dot_general | solution.py:152
  120.2 10.1 %fusion.9 = bf16[1,512,2048]{2,1,0:T(8,128)(2,1)} fusion(bf16[1,896,2048]{2,1,0:T(8,128)(2,1)} %param.19, f32[512,896]{1,0:T(8,128)} %fusion.4, bf16[512,2048]{1,0:T(8,128)(2,1)} %bitcast.53, bf16[1,2048,896]{2,1,0:T(8,128)(2,1)} %param.18), kind=kOutput, calls=%fused_computation.8 | convolution fusion | flops 3761897472 | bytes 13369344 | tf_op jit(solution)/shard_map/xnf,xfd->xnd/dot_general | solution.py:155
  130.3 0.0 reduce-scatter.2.cloned.1.call-update
  130.3 1.3 collective-permute-start.1
  131.6 20.9 %collective-permute-done.1 = bf16[384,512]{1,0:T(8,128)(2,1)S(1)} collective-permute-done((bf16[384,512]{1,0:T(8,128)(2,1)S(1)}, bf16[384,512]{1,0:T(8,128)(2,1)S(1)}, u32[]{:S(2)}, u32[]{:S(2)}) %collective-permute-start.1) | collective-permute-done | bytes 393248 | tf_op jit(solution)/shard_map/ppermute | solution.py:149
  152.6 14.2 %reduce-scatter.2.cloned.1.call-done = bf16[1,512,512]{2,1,0:T(8,128)(2,1)} async-done(((bf16[1,512,2048]{2,1,0:T(8,128)(2,1)}), bf16[1,512,512]{2,1,0:T(8,128)(2,1)}) %reduce-scatter.2.cloned.1.call-update) | async-done | bytes 524304 | tf_op jit(solution)/shard_map/reduce_scatter | solution.py:158
  166.7 1.9 copy.33
  168.6 5.4 %all-to-all-start.1 = ((bf16[1,4,8,16,512]{4,3,1,0,2:T(8,128)(2,1)}), bf16[1,4,8,16,512]{4,3,1,0,2:T(8,128)(2,1)S(1)}, u32[]{:S(2)}, u32[]{:S(2)}) async-start(bf16[1,4,8,16,512]{4,3,1,0,2:T(8,128)(2,1)} %copy.33), calls=%async_computation.2 | async-start | bytes 1048576 | tf_op jit(solution)/shard_map/all_to_all | solution.py:162
  174.1 0.1 mul.84
  174.2 0.1 copy.34
  174.3 1.0 add_convert_fusion
  175.3 11.5 %all-to-all-done.1 = bf16[1,4,8,16,512]{4,3,1,0,2:T(8,128)(2,1)S(1)} async-done(((bf16[1,4,8,16,512]{4,3,1,0,2:T(8,128)(2,1)}), bf16[1,4,8,16,512]{4,3,1,0,2:T(8,128)(2,1)S(1)}, u32[]{:S(2)}, u32[]{:S(2)}) %all-to-all-start.1) | async-done | bytes 524320 | tf_op jit(solution)/shard_map/all_to_all | solution.py:162
  186.8 1.2 gather_fusion
  188.0 0.3 reshape.140
  188.3 0.7 multiply_reduce_fusion
  189.1 7.3 %all_gather.27 = bf16[128,2048]{1,0:T(8,128)(2,1)S(1)} all-gather(bf16[128,512]{1,0:T(8,128)(2,1)S(1)} %multiply_reduce_fusion), channel_id=1, replica_groups=mesh['ep'=8,'tp'=4] {'tp'}, dimensions={1}, use_global_device_ids=true | all-gather | bytes 655360 | tf_op jit(solution)/shard_map/all_gather | solution.py:167
  196.3 0.8 copy.37
  (21 shorter events, 0.1 us)
Async XLA Ops:
  7.2 13.7 %copy-start.3 = (bf16[128,2048]{1,0:T(8,128)(2,1)S(1)}, bf16[128,2048]{1,0:T(8,128)(2,1)}, u32[]{:S(2)}) copy-start(bf16[128,2048]{1,0:T(8,128)(2,1)} %param.15) | copy-start | bytes 1572868
  7.2 21.1 %copy-start.2 = (bf16[384,512]{1,0:T(8,128)(2,1)S(1)}, bf16[384,512]{1,0:T(8,128)(2,1)}, u32[]{:S(2)}) copy-start(bf16[384,512]{1,0:T(8,128)(2,1)} %q_ref.1) | copy-start | bytes 1179652
  7.2 43.4 %all-gather.7.cloned.1.call-start = ((), (), s32[]{:S(2)}) async-start(), calls=%async_computation.3 | async-start | bytes 1966080 | tf_op jit(solution)/shard_map/all_gather | solution.py:65
  7.9 79.9 %all-gather.9.cloned.1.call-start = ((), (), s32[]{:S(2)}) async-start(), calls=%async_computation.4 | async-start | bytes 1966080 | tf_op jit(solution)/shard_map/all_gather | solution.py:65
  22.8 24.0 %all-to-all-start = ((bf16[8,16,2048]{2,1,0:T(8,128)(2,1)}), bf16[8,16,2048]{2,1,0:T(8,128)(2,1)S(1)}, u32[]{:S(2)}, u32[]{:S(2)}) async-start(bf16[8,16,2048]{2,1,0:T(8,128)(2,1)} %bitcast.6), calls=%async_computation | async-start | bytes 1048576 | tf_op jit(solution)/shard_map/all_to_all | solution.py:142
  28.2 85.7 %all-gather.11.cloned.1.call-start = ((), (), s32[]{:S(2)}) async-start(), calls=%async_computation.6 | async-start | bytes 2621440 | tf_op jit(solution)/shard_map/all_gather | solution.py:146
  28.2 18.5 %collective-permute-start = (bf16[384,512]{1,0:T(8,128)(2,1)S(1)}, bf16[384,512]{1,0:T(8,128)(2,1)S(1)}, u32[]{:S(2)}, u32[]{:S(2)}) collective-permute-start(bf16[384,512]{1,0:T(8,128)(2,1)S(1)} %copy-done.2), channel_id=1, source_target_pairs={{16,0},{20,4},{24,8},{28,12},{17,1},{21,5},{25,9},{29,13},{18,2},{... | collective-permute-start | bytes 1179656 | tf_op jit(solution)/shard_map/ppermute | solution.py:114
  46.8 41.1 %copy-start.4 = (bf16[8,16,2048]{2,1,0:T(8,128)(2,1)}, bf16[8,16,2048]{2,1,0:T(8,128)(2,1)S(1)}, u32[]{:S(2)}) copy-start(bf16[8,16,2048]{2,1,0:T(8,128)(2,1)S(1)} %all-to-all-done) | copy-start | bytes 1572868
  87.9 78.9 %reduce-scatter.2.cloned.1.call-start = ((), (), s32[]{:S(2)}) async-start(), calls=%async_computation.5 | async-start | bytes 2621440 | tf_op jit(solution)/shard_map/reduce_scatter | solution.py:158
  88.0 1.4 copy-start
  89.4 1.4 copy-start.1
  130.3 43.9 %copy-start.5 = (f32[128,2]{0,1:T(2,128)S(1)}, f32[128,2]{0,1:T(2,128)}, u32[]{:S(2)}) copy-start(f32[128,2]{0,1:T(2,128)} %param.21) | copy-start | bytes 3076
  130.3 22.2 %collective-permute-start.1 = (bf16[384,512]{1,0:T(8,128)(2,1)S(1)}, bf16[384,512]{1,0:T(8,128)(2,1)S(1)}, u32[]{:S(2)}, u32[]{:S(2)}) collective-permute-start(bf16[384,512]{1,0:T(8,128)(2,1)S(1)} %get-tuple-element.25), channel_id=1, source_target_pairs={{0,16},{4,20},{8,24},{12,28},{1,17},{5,21},{9,25},{13,29},{2,18},{... | collective-permute-start | bytes 1179656 | tf_op jit(solution)/shard_map/ppermute | solution.py:149
  168.6 18.2 %all-to-all-start.1 = ((bf16[1,4,8,16,512]{4,3,1,0,2:T(8,128)(2,1)}), bf16[1,4,8,16,512]{4,3,1,0,2:T(8,128)(2,1)S(1)}, u32[]{:S(2)}, u32[]{:S(2)}) async-start(bf16[1,4,8,16,512]{4,3,1,0,2:T(8,128)(2,1)} %copy.33), calls=%async_computation.2 | async-start | bytes 1048576 | tf_op jit(solution)/shard_map/all_to_all | solution.py:162
Sparse Core Ops, SparseCore 0:
  9.5 40.9 all-gather.6
  52.1 35.6 all-gather.8
  90.0 23.8 all-gather.10
  130.4 36.2 reduce-scatter.1
